TPU v7x, 128 devices: a whole 4x4x4 slice. The times are simulated.
128 devices in a mesh: sp: 32 (over z, y, core), tp: 4 (over x).
Axes of the slice: x: 4, y: 4, z: 4, core: 2. Of those that a mesh axis runs over, the one named last changes fastest.
Arguments:
- layer_source: bfloat16 [32768, 2048], P(('sp', 'tp')), may hold values from -6 to 6
- broad_probe_tensor: bfloat16 [32768, 512], P('sp', 'tp'), may hold values from -6 to 6
- broad_retention_preact: bfloat16 [32768, 512], P('sp', 'tp'), may hold values from -6 to 6
- broad_floor_margin: float32 [512], P('tp'), may hold values from 9.1552734e-06 to 0.12
- slim_probe_tensor: bfloat16 [32768, 256], P('sp', 'tp'), may hold values from -6 to 6
- slim_retention_preact: bfloat16 [32768, 256], P('sp', 'tp'), may hold values from -6 to 6
- slim_floor_margin: float32 [256], P('tp'), may hold values from 9.1552734e-06 to 0.12
- branch_content_tensor: bfloat16 [2, 32768, 512], P(None, 'sp', 'tp'), may hold values from -6 to 6
- emitted_switch_preact: bfloat16 [2, 32768, 512], P(None, 'sp', 'tp'), may hold values from -6 to 6
- extra_log_fades: float32 [2, 32768, 4], P(None, 'sp', 'tp'), may hold values from -1.4 to 0
- channel_norm_scale: float32 [128], replicated, may hold values from 0.1 to 1.9
- emission_projection: bfloat16 [2, 512, 2048], replicated, may hold values from -0.1875 to 0.1875
- mlp_norm_scale: float32 [2048], replicated, may hold values from 0.1 to 1.9
- switch_projection: bfloat16 [2048, 5632], P('sp', 'tp'), may hold values from -0.125 to 0.125
- expand_projection: bfloat16 [2048, 5632], P('sp', 'tp'), may hold values from -0.125 to 0.125
- shrink_projection: bfloat16 [5632, 2048], P('tp', 'sp'), may hold values from -0.078125 to 0.078125
Outputs:
- layer_out: bfloat16 [32768, 2048], P(('sp', 'tp'))
All inputs are finite; a program needn't handle non-finite values.
Results may differ from a plain program's by a relative error of at most 0.0095.
Values may be sent and summed in bfloat16 or wider, within the bound.
A program may use at most 192 MiB of HBM per device.

v0:
```python
import jax
import jax.numpy as jnp
from jax import lax
from jax.experimental import pallas as pl
from jax.experimental.pallas import tpu as pltpu
from jax.sharding import Mesh
from jax.sharding import PartitionSpec as P

BRANCH_CHANNELS = 4
BLOCK = 64
SP = ("sp_0", "sp_1", "sp_2")
SP_TP = ("sp_0", "sp_1", "sp_2", "tp")


EPSILON = 1e-06
EXACT_PRECISION = lax.Precision.HIGHEST


def filled_with(value, identity):
    return jax.tree.map(
        lambda part, zero: jnp.zeros_like(part) + jnp.asarray(zero, part.dtype), value, identity
    )


def collected_together(value, axis):
    leaves = jax.tree.leaves(value)
    turns = sorted(range(len(leaves)), key=lambda k: -leaves[k].size)
    width = (1, *leaves[turns[0]].shape)[-1]
    lines = [
        jnp.pad(leaves[k].reshape(-1), (0, -leaves[k].size % width)).reshape(-1, width)
        for k in turns
    ]
    both, at, found = (lax.all_gather(jnp.concatenate(lines), axis), 0, {})
    for k, line in zip(turns, lines):
        share = both[:, at : at + len(line)].reshape(len(both), -1)
        found[k] = share[:, : leaves[k].size].reshape(-1, *leaves[k].shape)
        at += len(line)
    numbers = iter(range(len(leaves)))
    return jax.tree.map(lambda _: found[next(numbers)], value)


def entering(value, axes, combine, identity):
    before = start = filled_with(value, identity)
    total = value
    for axis in reversed(axes):
        count, mine = (lax.axis_size(axis), lax.axis_index(axis))
        pieces = collected_together(total, axis)
        inside, total = (start, start)
        for k in range(count):
            passed = k < mine
            total = combine(total, jax.tree.map(lambda part: part[k], pieces))
            inside = jax.tree.map(lambda new, old: jnp.where(passed, new, old), total, inside)
        before = combine(inside, before)
    return before


def in_order(parts, dim):
    parts = jnp.moveaxis(parts, 0, dim)
    shape = parts.shape
    return parts.reshape(*shape[:dim], shape[dim] * shape[dim + 1], *shape[dim + 2 :])


def sent_to_all(value, axis):
    count = lax.axis_size(axis)
    return lax.all_to_all(
        jnp.broadcast_to(value[None], (count, *value.shape)), axis, 0, 0, tiled=True
    )


def collect(value, axis, dim):
    return in_order(sent_to_all(value, axis), dim)


def centred_block(query, key, value, prefix, mask, state):
    half = BLOCK // 2
    middle, total = (prefix[half - 1 : half, :], prefix[BLOCK - 1 : BLOCK, :])
    query_in = query * jnp.exp(prefix - middle)
    key_in = key * jnp.exp(middle - prefix)
    scores = lax.dot_general(
        query_in.astype(jnp.bfloat16),
        key_in.astype(jnp.bfloat16),
        (((1,), (1,)), ((), ())),
        preferred_element_type=jnp.float32,
    )
    scores = jnp.where(mask, scores, 0.0).astype(jnp.bfloat16)
    inside = jnp.dot(scores, value, preferred_element_type=jnp.float32)
    reach = query_in * jnp.exp(middle)
    earlier = lax.dot_general(
        reach.astype(jnp.bfloat16),
        state.astype(jnp.bfloat16),
        (((1,), (1,)), ((), ())),
        preferred_element_type=jnp.float32,
    )
    leaving = (key_in * jnp.exp(total - middle)).astype(jnp.bfloat16)
    state = state * jnp.exp(total) + lax.dot_general(
        value, leaving, (((0,), (0,)), ((), ())), preferred_element_type=jnp.float32
    )
    return (inside + earlier, reach, total, state)


def recurrence_kernel(
    wide_query,
    wide_forget,
    wide_gap,
    narrow_query,
    narrow_forget,
    narrow_gap,
    values,
    fades,
    wide_out,
    wide_reach,
    wide_state,
    wide_log,
    narrow_out,
    narrow_reach,
    narrow_state,
    narrow_log,
):
    rows = lax.broadcasted_iota(jnp.int32, (BLOCK, BLOCK), 0)
    columns = lax.broadcasted_iota(jnp.int32, (BLOCK, BLOCK), 1)
    mask = rows >= columns
    ones = jnp.where(mask, 1.0, 0.0)
    groups = (
        (wide_query, wide_forget, wide_gap, wide_out, wide_reach),
        (narrow_query, narrow_forget, narrow_gap, narrow_out, narrow_reach),
    )

    def advance(block, carried):
        at = pl.ds(pl.multiple_of(block * BLOCK, BLOCK), BLOCK)
        left = []
        for g in range(2):
            query_ref, forget_ref, gap_ref, out_ref, reach_ref = groups[g]
            state, running = carried[g]
            key = gap_ref[...] * jax.nn.sigmoid(-forget_ref[at, :].astype(jnp.float32))
            decay = jnp.log1p(-key) + fades[g, at, :]
            query = jax.nn.silu(query_ref[at, :].astype(jnp.float32)) * key.shape[1] ** (-0.5)
            prefix = jnp.dot(
                ones, decay, preferred_element_type=jnp.float32, precision=EXACT_PRECISION
            )
            out, reach, total, state = centred_block(
                query, key, values[g, at, :], prefix, mask, state
            )
            out_ref[at, :] = out
            reach_ref[at, :] = (reach * jnp.exp(running)).astype(jnp.bfloat16)
            left.append((state, running + total))
        return tuple(left)

    start = tuple(
        (
            jnp.zeros((values.shape[2], group[0].shape[1]), jnp.float32),
            jnp.zeros((1, group[0].shape[1]), jnp.float32),
        )
        for group in groups
    )
    wide, narrow = lax.fori_loop(0, wide_query.shape[0] // BLOCK, advance, start, unroll=4)
    wide_state[...], wide_log[...] = wide
    narrow_state[...], narrow_log[...] = narrow


def local_recurrence(wide_query, wide_forget, wide_gap, narrow_query, narrow_forget, narrow_gap, values, fades):
    length, width = (wide_query.shape[0], values.shape[2])
    vmem = pl.BlockSpec(memory_space=pltpu.VMEM)
    shapes = []
    for query in (wide_query, narrow_query):
        keys = query.shape[1]
        shapes += [
            jax.ShapeDtypeStruct((length, width), jnp.float32),
            jax.ShapeDtypeStruct((length, keys), jnp.bfloat16),
            jax.ShapeDtypeStruct((width, keys), jnp.float32),
            jax.ShapeDtypeStruct((1, keys), jnp.float32),
        ]
    return pl.pallas_call(
        recurrence_kernel,
        out_shape=tuple(shapes),
        in_specs=[vmem] * 8,
        out_specs=(vmem,) * 8,
        cost_estimate=pl.CostEstimate(flops=10**10, bytes_accessed=4 * 10**6, transcendentals=10**6),
    )(
        wide_query,
        wide_forget,
        wide_gap.reshape(1, -1),
        narrow_query,
        narrow_forget,
        narrow_gap.reshape(1, -1),
        values,
        fades,
    )


def head_norm(output_rows, channel_norm_scale, gate_rows):
    inverse = lax.rsqrt(jnp.mean(output_rows * output_rows, axis=2, keepdims=True) + EPSILON)
    normed = (output_rows * inverse * channel_norm_scale).reshape(output_rows.shape[0], -1)
    return (normed * jax.nn.silu(gate_rows.astype(jnp.float32))).astype(jnp.bfloat16)


def combine(earlier, later):
    wide_early, wide_state_early, narrow_early, narrow_state_early = earlier
    wide_late, wide_state_late, narrow_late, narrow_state_late = later
    return (
        wide_early + wide_late,
        jnp.exp(wide_late) * wide_state_early + wide_state_late,
        narrow_early + narrow_late,
        jnp.exp(narrow_late) * narrow_state_early + narrow_state_late,
    )


def local(
    layer_source,
    broad_probe_tensor,
    broad_retention_preact,
    broad_floor_margin,
    slim_probe_tensor,
    slim_retention_preact,
    slim_floor_margin,
    branch_content_tensor,
    emitted_switch_preact,
    extra_log_fades,
    channel_norm_scale,
    emission_projection,
    mlp_norm_scale,
    switch_projection,
    expand_projection,
    shrink_projection,
):
    tp_count = lax.axis_size("tp")
    row_count = layer_source.shape[0]
    gate_full = lax.all_gather(switch_projection, SP, axis=0, tiled=True)
    up_full = lax.all_gather(expand_projection, SP, axis=0, tiled=True)
    down_full = lax.all_gather(shrink_projection.T, SP, axis=0, tiled=True)
    found = local_recurrence(
        broad_probe_tensor,
        broad_retention_preact,
        broad_floor_margin,
        slim_probe_tensor,
        slim_retention_preact,
        slim_floor_margin,
        branch_content_tensor,
        extra_log_fades,
    )
    wide_out, wide_reach, wide_state, wide_log, narrow_out, narrow_reach, narrow_state, narrow_log = found
    identity = jax.tree.map(jnp.zeros_like, (wide_log, wide_state, narrow_log, narrow_state))
    carried = entering((wide_log, wide_state, narrow_log, narrow_state), SP, combine, identity)
    mixed_parts = []
    for g, (output_rows, reach, state) in enumerate(
        ((wide_out, wide_reach, carried[1]), (narrow_out, narrow_reach, carried[3]))
    ):
        output_rows = output_rows + lax.dot_general(
            reach,
            state.astype(jnp.bfloat16),
            (((1,), (1,)), ((), ())),
            preferred_element_type=jnp.float32,
        )
        mixed_parts.append(
            head_norm(output_rows[:, None, :], channel_norm_scale, emitted_switch_preact[g])
        )
    mixed = jnp.concatenate(mixed_parts, axis=1)
    group_width = branch_content_tensor.shape[2]
    model_width = emission_projection.shape[2]
    regrouped = lax.all_to_all(mixed, "tp", split_axis=0, concat_axis=1, tiled=True)
    shaped = regrouped.reshape(row_count, tp_count, 2, group_width)
    branch = jnp.einsum(
        "rtgc,gtcd->rd",
        shaped,
        emission_projection.reshape(2, tp_count, group_width, model_width),
        preferred_element_type=jnp.float32,
    )
    updated = layer_source.astype(jnp.float32) + branch
    inverse = lax.rsqrt(jnp.mean(updated * updated, axis=1, keepdims=True) + EPSILON)
    normed = (updated * inverse * mlp_norm_scale).astype(jnp.bfloat16)
    row_piece = collect(normed, "tp", 0)
    gate_part = jnp.dot(row_piece, gate_full, preferred_element_type=jnp.float32)
    up_part = jnp.dot(row_piece, up_full, preferred_element_type=jnp.float32)
    hidden = (jax.nn.silu(gate_part) * up_part).astype(jnp.bfloat16)
    ffn_sum = lax.psum_scatter(
        lax.dot_general(
            hidden, down_full, (((1,), (1,)), ((), ())), preferred_element_type=jnp.float32
        ).astype(jnp.bfloat16),
        "tp",
        scatter_dimension=0,
        tiled=True,
    ).astype(jnp.float32)
    return (updated + 0.5 * ffn_sum).astype(jnp.bfloat16)


def solution(mesh):
    torus = Mesh(mesh.devices.reshape(4, 4, 2, mesh.shape["tp"]), ("sp_0", "sp_1", "sp_2", "tp"))
    placed = (
        P(SP_TP, None),
        P(SP, "tp"),
        P(SP, "tp"),
        P("tp"),
        P(SP, "tp"),
        P(SP, "tp"),
        P("tp"),
        P(None, SP, "tp"),
        P(None, SP, "tp"),
        P(None, SP, "tp"),
        P(),
        P(),
        P(),
        P(SP, "tp"),
        P(SP, "tp"),
        P("tp", SP),
    )
    return jax.shard_map(
        local, mesh=torus, in_specs=placed, out_specs=P(SP_TP, None), check_vma=False
    )
```

profile of v0, /device:TPU:1, one launch (start us, length us, event | category | flops | bytes accessed | tf_op | source)
XLA Modules:
  0.0 238.1 jit_solution(414650234573479791)
XLA Ops:
  6.5 0.7 all-gather.10.cloned.1.call-update
  7.3 0.7 all-gather.12.cloned.1.call-update
  8.1 0.7 all-gather.14.cloned.1.call-update
  8.8 2.0 copy.48.fades
  10.8 1.8 copy.46.narrow_query
  12.6 1.8 copy.47.narrow_forget
  14.4 10.5 %shard_map.154 = (f32[1024,128]{1,0:T(8,128)}, bf16[1024,128]{1,0:T(8,128)(2,1)}, f32[128,128]{1,0:T(8,128)}, f32[1,128]{1,0:T(1,128)}, f32[1024,128]{1,0:T(8,12...) custom-call(bf16[1024,128]{1,0:T(8,128)(2,1)} %wide_query.1, bf16[1024,128]{1,0:T(8,128)(2,1)} %wide_forget.1, ...), custom_call_target="tpu_custom_call" | custom-call | flops 10000000000 | bytes 4000000 | tf_op jit(solution)/shard_map/pallas_call | solution.py:172
  24.9 1.1 reshape.430
  26.0 0.6 pad_bitcast_fusion.2
  26.6 0.9 maximum_bitcast_fusion
  27.4 3.0 %all-gather.3 = f32[2,194,128]{2,1,0:T(8,128)S(1)} all-gather(f32[1,194,128]{2,1,0:T(8,128)S(1)} %maximum_bitcast_fusion), channel_id=2, replica_groups=mesh['sp_0'=4,'sp_1'=4,'sp_2'=2,'tp'=4] {'sp_2'}, dimensions={0}, use_global_device_ids=true | all-gather | bytes 297984 | tf_op jit(solution)/shard_map/all_gather | solution.py:33
  30.5 0.1 mul.380
  30.5 0.1 mul.385
  30.7 11.2 %all-gather.4 = f32[4,194,128]{2,1,0:T(8,128)S(1)} all-gather(f32[1,194,128]{2,1,0:T(8,128)S(1)} %maximum_bitcast_fusion.1), channel_id=3, replica_groups=mesh['sp_0'=4,'sp_1'=4,'sp_2'=2,'tp'=4] {'sp_1'}, dimensions={0}, use_global_device_ids=true | all-gather | bytes 496640 | tf_op jit(solution)/shard_map/all_gather | solution.py:33
  41.8 0.5 fusion.85
  42.4 0.6 fusion.84
  43.1 0.1 mul.404
  43.2 0.1 mul.408
  43.3 0.1 mul.413
  43.4 0.2 copy-done.14
  43.5 0.1 mul.400
  43.7 14.0 %all-gather.5 = f32[4,194,128]{2,1,0:T(8,128)S(1)} all-gather(f32[1,194,128]{2,1,0:T(8,128)S(1)} %maximum_bitcast_fusion.2), channel_id=4, replica_groups=mesh['sp_0'=4,'sp_1'=4,'sp_2'=2,'tp'=4] {'sp_0'}, dimensions={0}, use_global_device_ids=true | all-gather | bytes 496640 | tf_op jit(solution)/shard_map/all_gather | solution.py:33
  58.1 0.6 fusion.94
  58.8 1.5 squeeze.114
  60.2 1.5 squeeze.115
  61.7 1.5 squeeze.116
  63.2 0.7 squeeze.117
  63.9 0.6 fusion.95
  64.5 1.5 squeeze.118
  65.9 0.7 squeeze.119
  66.6 0.7 exponential_bitcast_fusion.1
  67.3 0.6 exponential_bitcast_fusion
  68.0 1.1 multiply_reduce_fusion.2
  69.1 1.5 multiply_reduce_fusion.1
  70.7 1.0 multiply_multiply_fusion.1
  71.7 0.1 fusion.10
  71.9 0.1 fusion.11
  72.1 10.7 %all_to_all.18 = bf16[4,256,256]{2,1,0:T(8,128)(2,1)S(1)} all-to-all(bf16[4,256,256]{2,1,0:T(8,128)(2,1)S(1)} %pad_maximum_fusion), channel_id=1, replica_groups=mesh['sp_0'=4,'sp_1'=4,'sp_2'=2,'tp'=4] {'tp'}, dimensions={0} | all-to-all | bytes 1048576 | tf_op jit(solution)/shard_map/all_to_all | solution.py:259
  82.8 0.2 copy.51
  83.0 3.9 %multiply_reduce_fusion = (f32[256]{0:T(256)S(1)}, f32[256,2048]{1,0:T(8,128)S(1)}) fusion(bf16[2,4,128,2048]{3,2,1,0:T(8,128)(2,1)} %bitcast.239, bf16[256,4,2,128]{0,3,2,1:T(8,128)(2,1)S(1)} %bitcast.242, bf16[256,2048]{1,0:T(8,128)(2,1)} %param.16), kind=kOutput, calls=%fused_computation.6 | convolution fusion | flops 1075838720 | bytes 7865344 | tf_op jit(solution)/shard_map/rtgc,gtcd->rd/dot_general | solution.py:261
  87.0 0.2 multiply_convert_fusion.1
  87.2 0.5 broadcast_in_dim.14
  87.7 46.8 %all_to_all.19 = bf16[4,256,2048]{2,1,0:T(8,128)(2,1)} all-to-all(bf16[4,256,2048]{2,1,0:T(8,128)(2,1)S(1)} %broadcast_in_dim.14), channel_id=1, replica_groups=mesh['sp_0'=4,'sp_1'=4,'sp_2'=2,'tp'=4] {'tp'}, dimensions={0} | all-to-all | bytes 8388608 | tf_op jit(solution)/shard_map/all_to_all | solution.py:65
  134.6 11.7 %fusion.96 = f32[1024,1408]{1,0:T(8,128)} fusion(bf16[1024,2048]{1,0:T(8,128)(2,1)} %bitcast.240, bf16[2048,1408]{1,0:T(8,128)(2,1)} %all-gather.10.cloned.1.call-done), kind=kOutput, calls=%fused_computation.179 | convolution fusion | flops 5905580032 | bytes 15728640 | tf_op jit(solution)/shard_map/dot_general | solution.py:271
  146.3 16.7 %all-gather.14.cloned.1.call-done = bf16[2048,1408]{1,0:T(8,128)(2,1)} async-done(((bf16[64,1408]{1,0:T(8,128)(2,1)}), bf16[2048,1408]{1,0:T(8,128)(2,1)}) %all-gather.14.cloned.1.call-update) | async-done | bytes 5767184 | tf_op jit(solution)/shard_map/all_gather | solution.py:229
  163.0 20.6 %convolution_convert_fusion = bf16[1024,2048]{1,0:T(8,128)(2,1)} fusion(bf16[2048,1408]{1,0:T(8,128)(2,1)} %all-gather.14.cloned.1.call-done, f32[1024,1408]{1,0:T(8,128)} %fusion.96, bf16[1024,2048]{1,0:T(8,128)(2,1)} %bitcast.241, bf16[2048,1408]{1,0:T(8,128)(2,1)} %all-gather.12.cloned.1.call-done), kind=kOutput, calls=%fused_computation.1 | convolution fusion | flops 11821907968 | bytes 25690112 | tf_op jit(solution)/shard_map/dot_general | solution.py:275
  183.6 45.4 %reduce-scatter.2.cloned.1.call-done = bf16[256,2048]{1,0:T(8,128)(2,1)} async-done(((bf16[1024,2048]{1,0:T(8,128)(2,1)}), bf16[256,2048]{1,0:T(8,128)(2,1)}) %reduce-scatter.2.cloned.1.call-update) | async-done | bytes 1048592 | tf_op jit(solution)/shard_map/reduce_scatter | solution.py:274
  229.0 2.5 %add_convert_fusion = bf16[256,2048]{1,0:T(8,128)(2,1)} fusion(f32[256,2048]{1,0:T(8,128)S(1)} %get-tuple-element.68, bf16[256,2048]{1,0:T(8,128)(2,1)} %reduce-scatter.2.cloned.1.call-done), kind=kLoop, calls=%fused_computation.4 | loop fusion | flops 2097152 | bytes 4194304 | tf_op jit(solution)/shard_map/convert_element_type | solution.py:282
  (68 shorter events, 0.8 us)
Async XLA Ops:
  6.5 128.0 %all-gather.10.cloned.1.call-start = ((), (), s32[]{:S(2)}) async-start(), calls=%async_computation.3 | async-start | bytes 5947392 | tf_op jit(solution)/shard_map/all_gather | solution.py:227
  7.3 139.0 %all-gather.12.cloned.1.call-start = ((), (), s32[]{:S(2)}) async-start(), calls=%async_computation.4 | async-start | bytes 5947392 | tf_op jit(solution)/shard_map/all_gather | solution.py:228
  8.0 155.0 %all-gather.14.cloned.1.call-start = ((), (), s32[]{:S(2)}) async-start(), calls=%async_computation.5 | async-start | bytes 5947392 | tf_op jit(solution)/shard_map/all_gather | solution.py:229
  8.7 220.3 %reduce-scatter.2.cloned.1.call-start = ((), (), s32[]{:S(2)}) async-start(), calls=%async_computation.6 | async-start | bytes 5242880 | tf_op jit(solution)/shard_map/reduce_scatter | solution.py:274
  24.9 43.1 %copy-start.1 = (f32[1024,128]{1,0:T(8,128)S(1)}, f32[1024,128]{1,0:T(8,128)}, u32[]{:S(2)}) copy-start(f32[1024,128]{1,0:T(8,128)} %get-tuple-element.13) | copy-start | bytes 1572868
  24.9 43.1 %copy-start.4 = (bf16[1024,128]{1,0:T(8,128)(2,1)S(1)}, bf16[1024,128]{1,0:T(8,128)(2,1)}, u32[]{:S(2)}) copy-start(bf16[1024,128]{1,0:T(8,128)(2,1)} %get-tuple-element.14) | copy-start | bytes 786436
  24.9 44.2 %copy-start.2 = (f32[1024,128]{1,0:T(8,128)S(1)}, f32[1024,128]{1,0:T(8,128)}, u32[]{:S(2)}) copy-start(f32[1024,128]{1,0:T(8,128)} %get-tuple-element.19) | copy-start | bytes 1572868
  24.9 44.2 %copy-start.3 = (bf16[1024,64]{1,0:T(8,128)(2,1)S(1)}, bf16[1024,64]{1,0:T(8,128)(2,1)}, u32[]{:S(2)}) copy-start(bf16[1024,64]{1,0:T(8,128)(2,1)} %get-tuple-element.20) | copy-start | bytes 393220
  24.9 45.8 %copy-start = (bf16[2,1024,128]{2,1,0:T(8,128)(2,1)S(1)}, bf16[2,1024,128]{2,1,0:T(8,128)(2,1)}, u32[]{:S(2)}) copy-start(bf16[2,1024,128]{2,1,0:T(8,128)(2,1)} %param.24) | copy-start | bytes 1572868
  30.4 13.2 %copy-start.9 = (f32[64]{0:T(128)}, f32[64]{0:T(128)S(1)}, u32[]{:S(2)}) copy-start(f32[64]{0:T(128)S(1)} %get-tuple-element.58) | copy-start | bytes 772
  30.4 13.2 %copy-start.10 = (f32[64]{0:T(128)}, f32[64]{0:T(128)S(1)}, u32[]{:S(2)}) copy-start(f32[64]{0:T(128)S(1)} %get-tuple-element.60) | copy-start | bytes 772
  43.0 0.6 copy-start.11
  43.0 0.7 copy-start.12
  43.0 0.7 copy-start.13
  43.0 0.5 copy-start.14
  43.0 14.8 %copy-start.6 = (f32[128]{0:T(128)}, f32[128]{0:T(128)S(1)}, u32[]{:S(2)}) copy-start(f32[128]{0:T(128)S(1)} %get-tuple-element.36) | copy-start | bytes 1540
  43.1 14.8 %copy-start.7 = (f32[128]{0:T(128)}, f32[128]{0:T(128)S(1)}, u32[]{:S(2)}) copy-start(f32[128]{0:T(128)S(1)} %get-tuple-element.37) | copy-start | bytes 1540
  43.1 14.8 %copy-start.8 = (f32[128]{0:T(128)}, f32[128]{0:T(128)S(1)}, u32[]{:S(2)}) copy-start(f32[128]{0:T(128)S(1)} %get-tuple-element.40) | copy-start | bytes 1540
  83.0 3.9 %copy-start.5 = (f32[2048]{0:T(1024)S(1)}, f32[2048]{0:T(1024)}, u32[]{:S(2)}) copy-start(f32[2048]{0:T(1024)} %param.28) | copy-start | bytes 24580
Sparse Core Ops, SparseCore 0:
  9.6 54.0 all-gather.9
  65.9 47.4 all-gather.11
  115.7 47.1 all-gather.13
  183.7 45.2 reduce-scatter.1
where the time goes:
time: 239 us; the launch traced here: 238 us
  blocking collectives  85.7 us (36%)
  waiting for transfers between devices  64.2 us (27%)
  matrix products  38.9 us (16%)
  local copies, waits for them, and re-layouts  18.8 us (8%)
  between operations  13.6 us (6%)
  Pallas kernels  10.5 us (4%)
  other arithmetic  6.24 us (3%)
    all_to_all x1, blocking collectives, sent_to_all(): lax.all_to_all(jnp.broadcast_to(value[None], (count, *value.shape)), axis...  46.8 us
    reduce_scatter x1, waiting for transfers between devices, local(): lax.psum_scatter(lax.dot_general(hidden, down_full, (((1,), (1,)), ((), (...  45.4 us
    all_gather x3, blocking collectives, collected_together(): both, at, found = (lax.all_gather(jnp.concatenate(lines), axis), 0, {})  28.2 us
    dot_general x1, matrix products, local(): lax.dot_general(hidden, down_full, (((1,), (1,)), ((), ())), preferred_el...  20.6 us
    all_gather x1, waiting for transfers between devices, local(): down_full = lax.all_gather(shrink_projection.T, SP, axis=0, tiled=True)  16.7 us
    dot_general x1, matrix products, local(): jnp.dot(row_piece, gate_full, preferred_element_type=jnp.float32)  11.7 us
    all_to_all x1, blocking collectives, local(): lax.all_to_all(mixed, 'tp', split_axis=0, concat_axis=1, tiled=True)  10.7 us
    pallas_call x1, Pallas kernels, local_recurrence(): pl.pallas_call(recurrence_kernel, out_shape=tuple(shapes), in_specs=[vmem...  10.5 us
  transfers between devices with their start and end apart: 4, of which 2 were waited for; matrix products, arithmetic and copies ran while one was open for 17% of the time, Pallas kernels for 4%

commit v1 on v0

v1 whole, which is shorter than its diff:
```python
import jax
import jax.numpy as jnp
from jax import lax
from jax.experimental import pallas as pl
from jax.experimental.pallas import tpu as pltpu
from jax.sharding import Mesh
from jax.sharding import PartitionSpec as P

BLOCK = 64
RING = 4
SP = ("sp_0", "sp_1", "sp_2")
SP_TP = ("sp_0", "sp_1", "sp_2", "tp")

EPSILON = 1e-06
EXACT_PRECISION = lax.Precision.HIGHEST
BF16 = jnp.bfloat16
F32 = jnp.float32
NT = (((1,), (1,)), ((), ()))
TN = (((0,), (0,)), ((), ()))
MESH = pl.DeviceIdType.MESH

ARRIVALS = (
    (3, 0, 0),
    (1, 0, 1),
    (0, 3, 0),
    (0, 1, 1),
    (3, 0, 1),
    (1, 0, 0),
    (0, 3, 1),
    (0, 1, 0),
    (2, 0, 0),
    (2, 0, 1),
    (3, 3, 0),
    (3, 1, 1),
    (1, 3, 0),
    (1, 1, 1),
    (3, 3, 1),
    (3, 1, 0),
    (0, 2, 0),
    (0, 2, 1),
    (1, 3, 1),
    (1, 1, 0),
    (2, 3, 0),
    (2, 1, 1),
    (2, 3, 1),
    (2, 1, 0),
    (3, 2, 0),
    (3, 2, 1),
    (1, 2, 0),
    (1, 2, 1),
    (2, 2, 0),
    (2, 2, 1),
)


def turn(value, step):
    return lax.rem(value + step, RING)


def dot(a, b, dims=(((1,), (0,)), ((), ())), precision=None):
    return lax.dot_general(a, b, dims, preferred_element_type=F32, precision=precision)


def combine(earlier, later):
    wide_early, narrow_early, wide_state_early, narrow_state_early = earlier
    wide_late, narrow_late, wide_state_late, narrow_state_late = later
    return (
        wide_early + wide_late,
        narrow_early + narrow_late,
        jnp.exp(wide_late) * wide_state_early + wide_state_late,
        jnp.exp(narrow_late) * narrow_state_early + narrow_state_late,
    )


def split_log(log):
    first = log.astype(BF16).astype(F32)
    second = (log - first).astype(BF16).astype(F32)
    return [first, second, log - first - second]


def store_state(ref, at, state):
    wide, narrow, wide_state, narrow_state = state
    ref[at, 0:128, :] = wide_state.astype(BF16)
    ref[at, 128:192, :] = narrow_state.astype(BF16)
    lines = split_log(wide) + split_log(narrow)
    lines.append(jnp.zeros((10, wide.shape[1]), F32))
    ref[at, 192:208, :] = jnp.concatenate(lines, axis=0).astype(BF16)


def load_state(ref, at):
    lines = ref[at, 192:208, :].astype(F32)
    wide = lines[0:1] + lines[1:2] + lines[2:3]
    narrow = lines[3:4] + lines[4:5] + lines[5:6]
    return (wide, narrow, ref[at, 0:128, :].astype(F32), ref[at, 128:192, :].astype(F32))


def selected(passed, new, old):
    return jax.tree.map(lambda a, b: jnp.where(passed, a, b), new, old)


def block_step(query, key, value, prefix, mask, state):
    half = BLOCK // 2
    middle, total = (prefix[half - 1 : half, :], prefix[BLOCK - 1 : BLOCK, :])
    query_in = query * jnp.exp(prefix - middle)
    key_in = key * jnp.exp(middle - prefix)
    scores = dot(query_in.astype(BF16), key_in.astype(BF16), NT)
    scores = jnp.where(mask, scores, 0.0).astype(BF16)
    inside = dot(scores, value)
    reach = query_in * jnp.exp(middle)
    earlier = dot(reach.astype(BF16), state.astype(BF16), NT)
    leaving = (key_in * jnp.exp(total - middle)).astype(BF16)
    state = state * jnp.exp(total) + dot(value, leaving, TN)
    return (inside + earlier, reach, total, state)


def layer_kernel(
    layer_source,
    wide_query,
    wide_forget,
    wide_gap,
    narrow_query,
    narrow_forget,
    narrow_gap,
    values,
    switches,
    fades,
    channel_norm_scale,
    emission,
    mlp_scale,
    gate_shard,
    up_shard,
    down_shard,
    layer_out,
    weights,
    sources,
    mixed,
    projection,
    updated,
    normed,
    hidden,
    partial,
    own_part,
    passing,
    landed,
    narrow_q,
    narrow_f,
    wide_out,
    narrow_out,
    wide_reach,
    narrow_reach,
    core_states,
    y_states,
    z_states,
    load_sem,
    w_send,
    w_recv,
    d_send,
    d_recv,
    x_send,
    x_recv,
    s_send,
    s_recv,
    r_send,
    r_recv,
):
    z, y, core, x = (lax.axis_index(name) for name in SP_TP)
    other = 1 - core
    rows, model = layer_source.shape
    length = wide_query.shape[0]
    ff = gate_shard.shape[1]
    depth = gate_shard.shape[0]
    sent = []

    def send(src, dst, send_sem, recv_sem, to):
        copy = pltpu.make_async_remote_copy(
            src_ref=src,
            dst_ref=dst,
            send_sem=send_sem,
            recv_sem=recv_sem,
            device_id=to,
            device_id_type=MESH,
        )
        copy.start()
        sent.append(copy)

    partner = {"sp_2": other}

    def arrived(ref, sem):
        pltpu.make_async_remote_copy(
            src_ref=ref,
            dst_ref=ref,
            send_sem=sem,
            recv_sem=sem,
            device_id=partner,
            device_id_type=MESH,
        ).wait_recv()

    def place(i, j, of_core):
        first = jnp.where(of_core == 0, y, z)
        second = jnp.where(of_core == 0, z, y)
        first, second = (turn(first, i), turn(second, j))
        return (
            jnp.where(of_core == 0, second, first),
            jnp.where(of_core == 0, first, second),
        )

    def slot(i, j, of_core):
        at_z, at_y = place(i, j, of_core)
        return at_z * 8 + at_y * 2 + of_core

    half_depth = depth // 2

    def shard(i, j, h, of_core):
        return weights.at[slot(i, j, of_core), pl.ds(h * half_depth, half_depth), :]

    def toward(i, j):
        at_z, at_y = place(i, j, core)
        return {"sp_0": at_z, "sp_1": at_y}

    def mark(i, j, h):
        return (i * 4 + j) * 2 + h

    counts = {"w": 0, "d": 0, "x": 0}

    def next_of(name):
        counts[name] += 1
        return counts[name] - 1

    def forward(i, j, h, step, landing):
        src = shard(i, j, h, core)
        send(src, src, w_send.at[next_of("w")], w_recv.at[mark(*landing, h)], toward(*step))

    def hand_over(i, j, h):
        src = shard(i, j, h, core)
        send(src, src, d_send.at[next_of("d")], d_recv.at[mark(i, j, h)], partner)

    def spread_second(i, h):
        forward(i, 0, h, (0, 1), (i, 3))
        forward(i, 0, h, (0, 3), (i, 1))

    def pump(events):
        for i, j, h in events:
            arrived(shard(i, j, h, core), w_recv.at[mark(i, j, h)])
            if j == 0:
                if (i, h) == (3, 0):
                    forward(i, 0, h, (1, 0), (2, 0))
                if (i, h) == (1, 1):
                    forward(i, 0, h, (3, 0), (2, 0))
                spread_second(i, h)
            else:
                if (j, h) == (3, 0):
                    forward(i, j, h, (0, 1), (i, 2))
                if (j, h) == (1, 1):
                    forward(i, j, h, (0, 3), (i, 2))
            hand_over(i, j, h)

    def x_piece(buffer, step, h):
        half = buffer.shape[1] // 2
        return buffer.at[turn(x, step), pl.ds(h * half, half), :]

    def x_forward(buffer, base, step, h, to, landing):
        src = x_piece(buffer, step, h)
        send(src, src, x_send.at[next_of("x")], x_recv.at[base + landing * 2 + h], {"tp": turn(x, to)})

    def x_wait(buffer, base, step, h):
        arrived(x_piece(buffer, step, h), x_recv.at[base + step * 2 + h])

    def x_start(buffer, base, h):
        x_forward(buffer, base, 0, h, 1, 3)
        x_forward(buffer, base, 0, h, 3, 1)

    def x_relay(buffer, base):
        x_wait(buffer, base, 3, 0)
        x_forward(buffer, base, 3, 0, 1, 2)
        x_wait(buffer, base, 1, 1)
        x_forward(buffer, base, 1, 1, 3, 2)

    def x_finish(buffer, base):
        for step, h in ((3, 1), (1, 0), (2, 0), (2, 1)):
            x_wait(buffer, base, step, h)

    me = slot(0, 0, core)
    loads = []

    def load(src, dst):
        copy = pltpu.make_async_copy(src, dst, load_sem.at[len(loads)])
        copy.start()
        loads.append(copy)

    for n in range(ff // 128):
        cols = pl.ds(n * 128, 128)
        load(gate_shard.at[:, cols], weights.at[me, :, pl.ds(n * 256, 128)])
        load(up_shard.at[:, cols], weights.at[me, :, pl.ds(n * 256 + 128, 128)])
    load(down_shard, weights.at[me, :, pl.ds(2 * ff, ff)])
    load(layer_source, sources.at[x])
    first_loads = len(loads)
    for t in range(RING):
        for g in range(2):
            load(emission.at[g, pl.ds(t * 128, 128), :], projection.at[t, pl.ds(g * 128, 128), :])

    barrier = pltpu.get_barrier_semaphore()
    pl.semaphore_signal(barrier, inc=1, device_id=partner, device_id_type=MESH)
    for name, here in (("sp_0", z), ("sp_1", y), ("tp", x)):
        for step in (1, 2, 3):
            pl.semaphore_signal(
                barrier, inc=1, device_id={name: turn(here, step)}, device_id_type=MESH
            )
    pl.semaphore_wait(barrier, 10)

    for copy in loads[:first_loads]:
        copy.wait()
    for h in range(2):
        forward(0, 0, h, (1, 0), (3, 0))
        forward(0, 0, 1 - h, (3, 0), (1, 0))
        forward(0, 0, h, (0, 1), (0, 3))
        forward(0, 0, 1 - h, (0, 3), (0, 1))
        x_forward(sources, 0, 0, h, 1, 3)
        x_forward(sources, 0, 0, 1 - h, 3, 1)
    for h in range(2):
        hand_over(0, 0, h)

    for n in range(length // 128):
        cols = pl.ds(n * 128, 128)
        narrow_q[cols, :] = narrow_query[:, cols].astype(F32).T
        narrow_f[cols, :] = narrow_forget[:, cols].astype(F32).T
    line = lax.broadcasted_iota(jnp.int32, (BLOCK, BLOCK), 0)
    column = lax.broadcasted_iota(jnp.int32, (BLOCK, BLOCK), 1)
    mask = line >= column
    ones = jnp.where(mask, 1.0, 0.0)
    groups = (
        (wide_query, wide_forget, wide_gap, wide_out, wide_reach),
        (narrow_q, narrow_f, narrow_gap, narrow_out, narrow_reach),
    )

    def advance(block, carried):
        at = pl.ds(pl.multiple_of(block * BLOCK, BLOCK), BLOCK)
        left = []
        for g in range(2):
            query_ref, forget_ref, gap_ref, out_ref, reach_ref = groups[g]
            state, running = carried[g]
            key = gap_ref[...] * jax.nn.sigmoid(-forget_ref[at, :].astype(F32))
            decay = jnp.log1p(-key)
            query = jax.nn.silu(query_ref[at, :].astype(F32)) * key.shape[1] ** (-0.5)
            faded = jnp.sum(ones * fades[g, pl.ds(block, 1), :], axis=1, keepdims=True)
            prefix = dot(ones, decay, precision=EXACT_PRECISION) + faded
            out, reach, total, state = block_step(query, key, values[g, at, :], prefix, mask, state)
            out_ref[at, :] = out
            reach_ref[at, :] = (reach * jnp.exp(running)).astype(BF16)
            left.append((state, running + total))
        return tuple(left)

    start = tuple(
        (
            jnp.zeros((values.shape[2], group[2].shape[1]), F32),
            jnp.zeros((1, group[2].shape[1]), F32),
        )
        for group in groups
    )
    (wide_state, wide_log), (narrow_state, narrow_log) = lax.fori_loop(
        0, length // BLOCK, advance, start, unroll=4
    )
    packed = jnp.concatenate([narrow_state[0:64], narrow_state[64:128]], axis=1)
    narrow_log = jnp.concatenate([narrow_log, narrow_log], axis=1)

    store_state(core_states, core, (wide_log, narrow_log, wide_state, packed))
    src = core_states.at[core]
    send(src, src, s_send.at[0], s_recv.at[0], partner)
    x_relay(sources, 0)
    arrived(core_states.at[other], s_recv.at[0])
    first = load_state(core_states, 0)
    nothing = jax.tree.map(jnp.zeros_like, first)
    entering = selected(core == 1, first, nothing)
    total = combine(first, load_state(core_states, 1))
    for base, ref, name, here in ((1, y_states, "sp_1", y), (5, z_states, "sp_0", z)):
        store_state(ref, here, total)
        src = ref.at[here]
        for step in (1, 3, 2):
            send(src, src, s_send.at[base + step - 1], s_recv.at[base + here], {name: turn(here, step)})
        if base == 5:
            pump(ARRIVALS[0:8])
        for step in (1, 3, 2):
            peer = turn(here, step)
            arrived(ref.at[peer], s_recv.at[base + peer])
        inside, total = (nothing, nothing)
        for k in range(RING):
            total = combine(total, load_state(ref, k))
            inside = selected(k < here, total, inside)
        entering = combine(inside, entering)
    _, _, wide_state, packed = entering
    narrow_state = jnp.concatenate([packed[:, 0:64], packed[:, 64:128]], axis=0).astype(BF16)
    wide_state = wide_state.astype(BF16)

    for n in range(RING):
        at = pl.ds(n * rows, rows)
        parts = []
        for g, (out_ref, reach_ref, state) in enumerate(
            ((wide_out, wide_reach, wide_state), (narrow_out, narrow_reach, narrow_state))
        ):
            out = out_ref[at, :] + dot(reach_ref[at, :], state, NT)
            inverse = lax.rsqrt(jnp.mean(out * out, axis=1, keepdims=True) + EPSILON)
            out = out * inverse * channel_norm_scale[...]
            parts.append((out * jax.nn.silu(switches[g, at, :].astype(F32))).astype(BF16))
        mixed[x, at, :] = jnp.concatenate(parts, axis=1)
        if n % 2 == 1:
            x_start(mixed, 8, n // 2)

    pump(ARRIVALS[8:22])
    x_relay(mixed, 8)
    pump(ARRIVALS[22:])
    x_finish(sources, 0)
    x_finish(mixed, 8)
    for copy in loads[first_loads:]:
        copy.wait()

    def emit(owner):
        at = pl.ds(pl.multiple_of(owner * rows, rows), rows)
        left = jnp.concatenate([mixed[t, at, :] for t in range(RING)], axis=1)

        def tile(n, squares):
            cols = pl.ds(pl.multiple_of(n * 512, 512), 512)
            found = dot(left, projection[:, :, cols].reshape(4 * 256, 512))
            found = found + sources[owner, :, cols].astype(F32)
            updated[:, cols] = found
            found = found * found
            return squares + (
                (found[:, 0:128] + found[:, 128:256]) + (found[:, 256:384] + found[:, 384:512])
            )

        squares = lax.fori_loop(0, model // 512, tile, jnp.zeros((rows, 128), F32))
        mean = jnp.sum(squares, axis=1, keepdims=True) / model
        inverse = lax.rsqrt(mean + EPSILON)

        def scale(n, carry):
            cols = pl.ds(pl.multiple_of(n * 512, 512), 512)
            normed[:, cols] = (updated[:, cols] * inverse * mlp_scale[:, cols]).astype(BF16)
            return carry

        lax.fori_loop(0, model // 512, scale, 0)

    def feed_forward(out_ref):
        def widen(n, carry):
            cols = pl.ds(pl.multiple_of(n * 256, 256), 256)
            both = dot(normed[...], weights[:, :, cols].reshape(model, 256))
            found = (jax.nn.silu(both[:, 0:128]) * both[:, 128:256]).astype(BF16)
            hidden[:, pl.ds(pl.multiple_of(n * 128, 128), 128)] = found
            return carry

        lax.fori_loop(0, ff // 128, widen, 0)

        def shrink(n, carry):
            cols = pl.ds(pl.multiple_of(n * 256, 256), 256)
            four = weights[pl.ds(n * 4, 4), :, pl.ds(2 * ff, ff)].reshape(256, ff)
            out_ref[:, cols] = dot(hidden[...], four, NT).astype(out_ref.dtype)
            return carry

        lax.fori_loop(0, model // 256, shrink, 0)

    half = rows // 2
    upper, lower = (pl.ds(0, half), pl.ds(half, half))

    emit(turn(x, 2))
    for i in range(RING):
        for j in range(RING):
            for h in range(2):
                arrived(shard(i, j, h, other), d_recv.at[mark(i, j, h)])
    feed_forward(partial.at[0])
    send(partial.at[0, upper], passing.at[0], r_send.at[0], r_recv.at[0], {"tp": turn(x, 1)})
    send(partial.at[0, lower], passing.at[1], r_send.at[1], r_recv.at[1], {"tp": turn(x, 3)})
    emit(turn(x, 1))
    feed_forward(partial.at[1])
    send(partial.at[1, lower], landed.at[0, lower], r_send.at[2], r_recv.at[2], {"tp": turn(x, 1)})
    arrived(passing.at[0], r_recv.at[0])
    partial[1, upper, :] = (
        partial[1, upper, :].astype(F32) + passing[0].astype(F32)
    ).astype(BF16)
    send(partial.at[1, upper], landed.at[0, upper], r_send.at[3], r_recv.at[3], {"tp": turn(x, 1)})
    emit(turn(x, 3))
    feed_forward(partial.at[2])
    send(partial.at[2, upper], landed.at[1, upper], r_send.at[4], r_recv.at[4], {"tp": turn(x, 3)})
    arrived(passing.at[1], r_recv.at[1])
    partial[2, lower, :] = (
        partial[2, lower, :].astype(F32) + passing[1].astype(F32)
    ).astype(BF16)
    send(partial.at[2, lower], landed.at[1, lower], r_send.at[5], r_recv.at[5], {"tp": turn(x, 3)})
    emit(x)
    feed_forward(own_part)
    for n, (k, part) in enumerate(((0, lower), (0, upper), (1, upper), (1, lower))):
        arrived(landed.at[k, part], r_recv.at[2 + n])

    def finish(n, carry):
        cols = pl.ds(pl.multiple_of(n * 256, 256), 256)
        summed = own_part[:, cols] + (landed[0, :, cols].astype(F32) + landed[1, :, cols].astype(F32))
        layer_out[:, cols] = (updated[:, cols] + 0.5 * summed).astype(BF16)
        return carry

    lax.fori_loop(0, model // 256, finish, 0)
    for copy in sent:
        copy.wait_send()


def local(
    layer_source,
    broad_probe_tensor,
    broad_retention_preact,
    broad_floor_margin,
    slim_probe_tensor,
    slim_retention_preact,
    slim_floor_margin,
    branch_content_tensor,
    emitted_switch_preact,
    extra_log_fades,
    channel_norm_scale,
    emission_projection,
    mlp_norm_scale,
    switch_projection,
    expand_projection,
    shrink_projection,
):
    rows, model = layer_source.shape
    length = broad_probe_tensor.shape[0]
    depth, ff = switch_projection.shape
    vmem = pl.BlockSpec(memory_space=pltpu.VMEM)
    far = pl.BlockSpec(memory_space=pl.ANY)
    dma = pltpu.SemaphoreType.DMA
    return pl.pallas_call(
        layer_kernel,
        out_shape=jax.ShapeDtypeStruct((rows, model), BF16),
        in_specs=[far] + [vmem] * 10 + [far, vmem, far, far, far],
        out_specs=vmem,
        scratch_shapes=[
            pltpu.VMEM((32, depth, 3 * ff), BF16),
            pltpu.VMEM((RING, rows, model), BF16),
            pltpu.VMEM((RING, length, 256), BF16),
            pltpu.VMEM((RING, 256, model), BF16),
            pltpu.VMEM((rows, model), F32),
            pltpu.VMEM((rows, model), BF16),
            pltpu.VMEM((rows, ff), BF16),
            pltpu.VMEM((3, rows, model), BF16),
            pltpu.VMEM((rows, model), F32),
            pltpu.VMEM((2, rows // 2, model), BF16),
            pltpu.VMEM((2, rows, model), BF16),
            pltpu.VMEM((length, 64), F32),
            pltpu.VMEM((length, 64), F32),
            pltpu.VMEM((length, 128), F32),
            pltpu.VMEM((length, 128), F32),
            pltpu.VMEM((length, 128), BF16),
            pltpu.VMEM((length, 64), BF16),
            pltpu.VMEM((2, 208, 128), BF16),
            pltpu.VMEM((RING, 208, 128), BF16),
            pltpu.VMEM((RING, 208, 128), BF16),
            dma((32,)),
            dma((30,)),
            dma((32,)),
            dma((32,)),
            dma((32,)),
            dma((12,)),
            dma((16,)),
            dma((9,)),
            dma((9,)),
            dma((6,)),
            dma((6,)),
        ],
        compiler_params=pltpu.CompilerParams(
            collective_id=0, has_side_effects=True, vmem_limit_bytes=62 * 1024 * 1024
        ),
    )(
        layer_source,
        broad_probe_tensor,
        broad_retention_preact,
        broad_floor_margin.reshape(1, -1),
        slim_probe_tensor.T,
        slim_retention_preact.T,
        slim_floor_margin.reshape(1, -1),
        branch_content_tensor,
        emitted_switch_preact,
        extra_log_fades.reshape(2, length // BLOCK, BLOCK),
        channel_norm_scale.reshape(1, -1),
        emission_projection,
        mlp_norm_scale.reshape(1, -1),
        switch_projection,
        expand_projection,
        shrink_projection.T,
    )


def solution(mesh):
    torus = Mesh(mesh.devices.reshape(4, 4, 2, mesh.shape["tp"]), SP_TP)
    placed = (
        P(SP_TP, None),
        P(SP, "tp"),
        P(SP, "tp"),
        P("tp"),
        P(SP, "tp"),
        P(SP, "tp"),
        P("tp"),
        P(None, SP, "tp"),
        P(None, SP, "tp"),
        P(None, SP, "tp"),
        P(),
        P(),
        P(),
        P(SP, "tp"),
        P(SP, "tp"),
        P("tp", SP),
    )
    return jax.shard_map(
        local, mesh=torus, in_specs=placed, out_specs=P(SP_TP, None), check_vma=False
    )
```

time: 239 us -> 127 us (0.53)
  Pallas kernels: 10.5 us -> 121 us
  blocking collectives: 85.7 us -> 0 us
  waiting for transfers between devices: 64.2 us -> 0 us
  matrix products: 38.9 us -> 0 us
  local copies, waits for them, and re-layouts: 18.8 us -> 2.99 us
  between operations: 13.6 us -> 0.01 us
  other arithmetic: 6.24 us -> 0.73 us
    pallas_call x1, Pallas kernels: 10.5 us -> 121 us  [local(): pl.pallas_call(layer_kernel, out_shape=jax.ShapeDtypeStruct((rows, model)...]
    all_to_all x2 -> x0, blocking collectives: 57.5 us -> none  [the longest x1 46.8 us: sent_to_all(): lax.all_to_all(jnp.broadcast_to(value[None], (count, *value.shape)), axis...]
    reduce_scatter x1 -> x0, waiting for transfers between devices: 45.4 us -> none  [local(): lax.psum_scatter(lax.dot_general(hidden, down_full, (((1,), (1,)), ((), (...]
    dot_general x5 -> x0, matrix products: 38.9 us -> none  [the longest x1 20.6 us: local(): lax.dot_general(hidden, down_full, (((1,), (1,)), ((), ())), preferred_el...]
    all_gather x3 -> x0, blocking collectives: 28.2 us -> none  [collected_together(): both, at, found = (lax.all_gather(jnp.concatenate(lines), axis), 0, {})]
    all_gather x3 -> x0, waiting for transfers between devices: 16.7 us -> none  [the longest x1 16.7 us: local(): down_full = lax.all_gather(shrink_projection.T, SP, axis=0, tiled=True)]
    squeeze x10 -> x0, local copies, waits for them, and re-layouts: 7.55 us -> none  [entering(): total = combine(total, jax.tree.map(lambda part: part[k], pieces))]
    unnamed x33 -> x1, local copies, waits for them, and re-layouts: 5.79 us -> 2.3 us
  transfers between devices with their start and end apart: 4 -> 0, of which waited for: 2 -> 0; matrix products, arithmetic and copies ran while one was open for 17% -> 0% of each run, Pallas kernels for 4% -> 0%
where the time goes in v1:
time: 127 us; the launch traced here: 125 us
  Pallas kernels  121 us (95%)
  local copies, waits for them, and re-layouts  2.99 us (2%)
    pallas_call x1, Pallas kernels, local(): pl.pallas_call(layer_kernel, out_shape=jax.ShapeDtypeStruct((rows, model)...  121 us

profile of v1, /device:TPU:1, one launch (start us, length us, event | category | flops | bytes accessed | tf_op | source)
XLA Modules:
  0.0 124.6 jit_solution(9990619067445313280)
XLA Ops:
  0.0 0.7 reduce
  0.7 0.7 reshape.17.fades
  1.4 120.9 %shard_map.154 = bf16[256,2048]{1,0:T(8,128)(2,1)} custom-call(bf16[256,2048]{1,0:T(8,128)(2,1)} %layer_source.1, bf16[1024,128]{1,0:T(8,128)(2,1)} %wide_query.1, bf16[1024,128]{1,0:T(8,128)(2,1)} %wide_forget.1, f32[1,128]{1,0:T(1,128)} %bitcast.11, bf16[64,1024]{1,0:T(8,128)(2,1)} %bitcast.8, bf16[64,1024]{1,0:T(8,128)(2,1)} %bitcast.9, ...), custom_call_target="tpu_custom_call" | custom-call | tf_op jit(solution)/shard_map/pallas_call | solution.py:525
  122.3 2.3 %copy.18 = bf16[256,2048]{1,0:T(8,128)(2,1)} copy(bf16[256,2048]{1,0:T(8,128)(2,1)} %shard_map.154) | data formatting | bytes 2097152

commit v2 on v1

--- a/solution.py
+++ b/solution.py
@@ -210,49 +210,71 @@
 
     half_depth = depth // 2
 
-    def shard(i, j, h, of_core):
-        return weights.at[slot(i, j, of_core), pl.ds(h * half_depth, half_depth), :]
+    columns_of = (pl.ds(0, 2 * ff), pl.ds(2 * ff, ff))
+
+    def shard(i, j, h, part, of_core):
+        lines = pl.ds(h * half_depth, half_depth)
+        return weights.at[slot(i, j, of_core), lines, columns_of[part]]
+
+    def shard_part(i, j, part, of_core):
+        return weights.at[slot(i, j, of_core), :, columns_of[part]]
 
     def toward(i, j):
         at_z, at_y = place(i, j, core)
         return {"sp_0": at_z, "sp_1": at_y}
 
-    def mark(i, j, h):
-        return (i * 4 + j) * 2 + h
-
-    counts = {"w": 0, "d": 0, "x": 0}
+    def mark(i, j, h, part):
+        return part * 32 + (i * 4 + j) * 2 + h
+
+    counts = {"w": 0, "x": 0}
 
     def next_of(name):
         counts[name] += 1
         return counts[name] - 1
 
-    def forward(i, j, h, step, landing):
-        src = shard(i, j, h, core)
-        send(src, src, w_send.at[next_of("w")], w_recv.at[mark(*landing, h)], toward(*step))
-
-    def hand_over(i, j, h):
-        src = shard(i, j, h, core)
-        send(src, src, d_send.at[next_of("d")], d_recv.at[mark(i, j, h)], partner)
-
-    def spread_second(i, h):
-        forward(i, 0, h, (0, 1), (i, 3))
-        forward(i, 0, h, (0, 3), (i, 1))
-
-    def pump(events):
-        for i, j, h in events:
-            arrived(shard(i, j, h, core), w_recv.at[mark(i, j, h)])
+    def forward(i, j, h, part, step, landing):
+        src = shard(i, j, h, part, core)
+        at = w_recv.at[mark(*landing, h, part)]
+        send(src, src, w_send.at[next_of("w")], at, toward(*step))
+
+    def hand_over(i, j, part):
+        src = shard_part(i, j, part, core)
+        k = part * 16 + i * 4 + j
+        send(src, src, d_send.at[k], d_recv.at[k], partner)
+
+    handed = {}
+
+    def pump(part, first, last):
+        for i, j, h in ARRIVALS[first:last]:
+            arrived(shard(i, j, h, part, core), w_recv.at[mark(i, j, h, part)])
             if j == 0:
                 if (i, h) == (3, 0):
-                    forward(i, 0, h, (1, 0), (2, 0))
+                    forward(i, 0, h, part, (1, 0), (2, 0))
                 if (i, h) == (1, 1):
-                    forward(i, 0, h, (3, 0), (2, 0))
-                spread_second(i, h)
+                    forward(i, 0, h, part, (3, 0), (2, 0))
+                forward(i, 0, h, part, (0, 1), (i, 3))
+                forward(i, 0, h, part, (0, 3), (i, 1))
             else:
                 if (j, h) == (3, 0):
-                    forward(i, j, h, (0, 1), (i, 2))
+                    forward(i, j, h, part, (0, 1), (i, 2))
                 if (j, h) == (1, 1):
-                    forward(i, j, h, (0, 3), (i, 2))
-            hand_over(i, j, h)
+                    forward(i, j, h, part, (0, 3), (i, 2))
+            handed[(i, j, part)] = handed.get((i, j, part), 0) + 1
+            if handed[(i, j, part)] == 2:
+                hand_over(i, j, part)
+
+    def start_weights(part):
+        for h in range(2):
+            forward(0, 0, h, part, (1, 0), (3, 0))
+            forward(0, 0, 1 - h, part, (3, 0), (1, 0))
+            forward(0, 0, h, part, (0, 1), (0, 3))
+            forward(0, 0, 1 - h, part, (0, 3), (0, 1))
+        hand_over(0, 0, part)
+
+    def wait_partner(part):
+        for i in range(RING):
+            for j in range(RING):
+                arrived(shard_part(i, j, part, other), d_recv.at[part * 16 + i * 4 + j])
 
     def x_piece(buffer, step, h):
         half = buffer.shape[1] // 2
@@ -265,9 +287,13 @@
     def x_wait(buffer, base, step, h):
         arrived(x_piece(buffer, step, h), x_recv.at[base + step * 2 + h])
 
-    def x_start(buffer, base, h):
-        x_forward(buffer, base, 0, h, 1, 3)
-        x_forward(buffer, base, 0, h, 3, 1)
+    def x_first(buffer, base):
+        x_forward(buffer, base, 0, 0, 1, 3)
+        x_forward(buffer, base, 0, 1, 3, 1)
+
+    def x_second(buffer, base):
+        x_forward(buffer, base, 0, 1, 1, 3)
+        x_forward(buffer, base, 0, 0, 3, 1)
 
     def x_relay(buffer, base):
         x_wait(buffer, base, 3, 0)
@@ -275,9 +301,13 @@
         x_wait(buffer, base, 1, 1)
         x_forward(buffer, base, 1, 1, 3, 2)
 
-    def x_finish(buffer, base):
-        for step, h in ((3, 1), (1, 0), (2, 0), (2, 1)):
-            x_wait(buffer, base, step, h)
+    def x_opposite(buffer, base):
+        x_wait(buffer, base, 2, 0)
+        x_wait(buffer, base, 2, 1)
+
+    def x_rest(buffer, base):
+        x_wait(buffer, base, 3, 1)
+        x_wait(buffer, base, 1, 0)
 
     me = slot(0, 0, core)
     loads = []
@@ -309,16 +339,8 @@
 
     for copy in loads[:first_loads]:
         copy.wait()
-    for h in range(2):
-        forward(0, 0, h, (1, 0), (3, 0))
-        forward(0, 0, 1 - h, (3, 0), (1, 0))
-        forward(0, 0, h, (0, 1), (0, 3))
-        forward(0, 0, 1 - h, (0, 3), (0, 1))
-        x_forward(sources, 0, 0, h, 1, 3)
-        x_forward(sources, 0, 0, 1 - h, 3, 1)
-    for h in range(2):
-        hand_over(0, 0, h)
-
+    start_weights(0)
+    x_first(sources, 0)
     for n in range(length // 128):
         cols = pl.ds(n * 128, 128)
         narrow_q[cols, :] = narrow_query[:, cols].astype(F32).T
@@ -332,22 +354,27 @@
         (narrow_q, narrow_f, narrow_gap, narrow_out, narrow_reach),
     )
 
-    def advance(block, carried):
-        at = pl.ds(pl.multiple_of(block * BLOCK, BLOCK), BLOCK)
-        left = []
-        for g in range(2):
-            query_ref, forget_ref, gap_ref, out_ref, reach_ref = groups[g]
-            state, running = carried[g]
-            key = gap_ref[...] * jax.nn.sigmoid(-forget_ref[at, :].astype(F32))
-            decay = jnp.log1p(-key)
-            query = jax.nn.silu(query_ref[at, :].astype(F32)) * key.shape[1] ** (-0.5)
-            faded = jnp.sum(ones * fades[g, pl.ds(block, 1), :], axis=1, keepdims=True)
-            prefix = dot(ones, decay, precision=EXACT_PRECISION) + faded
-            out, reach, total, state = block_step(query, key, values[g, at, :], prefix, mask, state)
-            out_ref[at, :] = out
-            reach_ref[at, :] = (reach * jnp.exp(running)).astype(BF16)
-            left.append((state, running + total))
-        return tuple(left)
+    def advance(pair, carried):
+        for b in range(2):
+            at = pl.ds(pl.multiple_of((pair * 2 + b) * BLOCK, BLOCK), BLOCK)
+            left = []
+            for g in range(2):
+                query_ref, forget_ref, gap_ref, out_ref, reach_ref = groups[g]
+                state, running = carried[g]
+                key = gap_ref[...] * jax.nn.sigmoid(-forget_ref[at, :].astype(F32))
+                decay = jnp.log1p(-key)
+                query = jax.nn.silu(query_ref[at, :].astype(F32)) * key.shape[1] ** (-0.5)
+                fade = fades[g, :, pl.ds(pl.multiple_of(pair * 2 * BLOCK, 2 * BLOCK), 2 * BLOCK)]
+                faded = jnp.sum(ones * fade[:, b * BLOCK : (b + 1) * BLOCK], axis=1, keepdims=True)
+                prefix = dot(ones, decay, precision=EXACT_PRECISION) + faded
+                out, reach, total, state = block_step(
+                    query, key, values[g, at, :], prefix, mask, state
+                )
+                out_ref[at, :] = out
+                reach_ref[at, :] = (reach * jnp.exp(running)).astype(BF16)
+                left.append((state, running + total))
+            carried = tuple(left)
+        return carried
 
     start = tuple(
         (
@@ -356,8 +383,11 @@
         )
         for group in groups
     )
+    pairs = length // (2 * BLOCK)
+    middle = lax.fori_loop(0, pairs // 2, advance, start, unroll=2)
+    pump(0, 0, 4)
     (wide_state, wide_log), (narrow_state, narrow_log) = lax.fori_loop(
-        0, length // BLOCK, advance, start, unroll=4
+        pairs // 2, pairs, advance, middle, unroll=2
     )
     packed = jnp.concatenate([narrow_state[0:64], narrow_state[64:128]], axis=1)
     narrow_log = jnp.concatenate([narrow_log, narrow_log], axis=1)
@@ -365,7 +395,6 @@
     store_state(core_states, core, (wide_log, narrow_log, wide_state, packed))
     src = core_states.at[core]
     send(src, src, s_send.at[0], s_recv.at[0], partner)
-    x_relay(sources, 0)
     arrived(core_states.at[other], s_recv.at[0])
     first = load_state(core_states, 0)
     nothing = jax.tree.map(jnp.zeros_like, first)
@@ -376,8 +405,11 @@
         src = ref.at[here]
         for step in (1, 3, 2):
             send(src, src, s_send.at[base + step - 1], s_recv.at[base + here], {name: turn(here, step)})
-        if base == 5:
-            pump(ARRIVALS[0:8])
+        if base == 1:
+            x_relay(sources, 0)
+        else:
+            start_weights(1)
+            pump(0, 4, 10)
         for step in (1, 3, 2):
             peer = turn(here, step)
             arrived(ref.at[peer], s_recv.at[base + peer])
@@ -401,25 +433,41 @@
             out = out * inverse * channel_norm_scale[...]
             parts.append((out * jax.nn.silu(switches[g, at, :].astype(F32))).astype(BF16))
         mixed[x, at, :] = jnp.concatenate(parts, axis=1)
-        if n % 2 == 1:
-            x_start(mixed, 8, n // 2)
-
-    pump(ARRIVALS[8:22])
+
+    x_first(mixed, 8)
+    x_second(mixed, 8)
+
+    pump(0, 10, 24)
     x_relay(mixed, 8)
-    pump(ARRIVALS[22:])
-    x_finish(sources, 0)
-    x_finish(mixed, 8)
+    x_second(sources, 0)
+    pump(0, 24, 30)
+    pump(1, 0, 18)
+    x_rest(mixed, 8)
+    x_opposite(mixed, 8)
+    x_opposite(sources, 0)
     for copy in loads[first_loads:]:
         copy.wait()
 
-    def emit(owner):
-        at = pl.ds(pl.multiple_of(owner * rows, rows), rows)
-        left = jnp.concatenate([mixed[t, at, :] for t in range(RING)], axis=1)
+    half = rows // 2
+    upper, lower = (pl.ds(0, half), pl.ds(half, half))
+
+    def emit(pieces):
+        def lines(owner, h):
+            return pl.ds(pl.multiple_of(owner * rows + h * half, half), half)
+
+        left = jnp.concatenate(
+            [
+                jnp.concatenate([mixed[t, lines(owner, h), :] for owner, h in pieces], axis=0)
+                for t in range(RING)
+            ],
+            axis=1,
+        )
 
         def tile(n, squares):
             cols = pl.ds(pl.multiple_of(n * 512, 512), 512)
             found = dot(left, projection[:, :, cols].reshape(4 * 256, 512))
-            found = found + sources[owner, :, cols].astype(F32)
+            source = [sources[owner, pl.ds(h * half, half), cols] for owner, h in pieces]
+            found = found + jnp.concatenate(source, axis=0).astype(F32)
             updated[:, cols] = found
             found = found * found
             return squares + (
@@ -437,7 +485,7 @@
 
         lax.fori_loop(0, model // 512, scale, 0)
 
-    def feed_forward(out_ref):
+    def widen_all():
         def widen(n, carry):
             cols = pl.ds(pl.multiple_of(n * 256, 256), 256)
             both = dot(normed[...], weights[:, :, cols].reshape(model, 256))
@@ -447,44 +495,50 @@
 
         lax.fori_loop(0, ff // 128, widen, 0)
 
+    def shrink_all(out_ref, passed=False):
         def shrink(n, carry):
             cols = pl.ds(pl.multiple_of(n * 256, 256), 256)
             four = weights[pl.ds(n * 4, 4), :, pl.ds(2 * ff, ff)].reshape(256, ff)
-            out_ref[:, cols] = dot(hidden[...], four, NT).astype(out_ref.dtype)
+            found = dot(hidden[...], four, NT)
+            if passed:
+                found = found + jnp.concatenate(
+                    [passing[0, :, cols], passing[1, :, cols]], axis=0
+                ).astype(F32)
+            out_ref[:, cols] = found.astype(out_ref.dtype)
             return carry
 
         lax.fori_loop(0, model // 256, shrink, 0)
 
-    half = rows // 2
-    upper, lower = (pl.ds(0, half), pl.ds(half, half))
-
-    emit(turn(x, 2))
-    for i in range(RING):
-        for j in range(RING):
-            for h in range(2):
-                arrived(shard(i, j, h, other), d_recv.at[mark(i, j, h)])
-    feed_forward(partial.at[0])
-    send(partial.at[0, upper], passing.at[0], r_send.at[0], r_recv.at[0], {"tp": turn(x, 1)})
-    send(partial.at[0, lower], passing.at[1], r_send.at[1], r_recv.at[1], {"tp": turn(x, 3)})
-    emit(turn(x, 1))
-    feed_forward(partial.at[1])
-    send(partial.at[1, lower], landed.at[0, lower], r_send.at[2], r_recv.at[2], {"tp": turn(x, 1)})
+    def send_sum(src, dst, k, step):
+        send(src, dst, r_send.at[k], r_recv.at[k], {"tp": turn(x, step)})
+
+    left_x, right_x = (turn(x, 3), turn(x, 1))
+
+    emit(((turn(x, 2), 0), (turn(x, 2), 1)))
+    pump(1, 18, 30)
+    wait_partner(0)
+    widen_all()
+    wait_partner(1)
+    shrink_all(partial.at[0])
+    send_sum(partial.at[0, upper], passing.at[0], 0, 1)
+    send_sum(partial.at[0, lower], passing.at[1], 1, 3)
+    emit(((right_x, 1), (left_x, 0)))
+    widen_all()
+    shrink_all(partial.at[1])
+    send_sum(partial.at[1, upper], landed.at[0, lower], 2, 1)
+    send_sum(partial.at[1, lower], landed.at[1, upper], 3, 3)
+    x_rest(sources, 0)
+    emit(((right_x, 0), (left_x, 1)))
+    widen_all()
     arrived(passing.at[0], r_recv.at[0])
-    partial[1, upper, :] = (
-        partial[1, upper, :].astype(F32) + passing[0].astype(F32)
-    ).astype(BF16)
-    send(partial.at[1, upper], landed.at[0, upper], r_send.at[3], r_recv.at[3], {"tp": turn(x, 1)})
-    emit(turn(x, 3))
-    feed_forward(partial.at[2])
-    send(partial.at[2, upper], landed.at[1, upper], r_send.at[4], r_recv.at[4], {"tp": turn(x, 3)})
     arrived(passing.at[1], r_recv.at[1])
-    partial[2, lower, :] = (
-        partial[2, lower, :].astype(F32) + passing[1].astype(F32)
-    ).astype(BF16)
-    send(partial.at[2, lower], landed.at[1, lower], r_send.at[5], r_recv.at[5], {"tp": turn(x, 3)})
-    emit(x)
-    feed_forward(own_part)
-    for n, (k, part) in enumerate(((0, lower), (0, upper), (1, upper), (1, lower))):
+    shrink_all(partial.at[2], passed=True)
+    send_sum(partial.at[2, upper], landed.at[0, upper], 4, 1)
+    send_sum(partial.at[2, lower], landed.at[1, lower], 5, 3)
+    emit(((x, 0), (x, 1)))
+    widen_all()
+    shrink_all(own_part)
+    for n, (k, part) in enumerate(((0, lower), (1, upper), (0, upper), (1, lower))):
         arrived(landed.at[k, part], r_recv.at[2 + n])
 
     def finish(n, carry):
@@ -549,8 +603,8 @@
             pltpu.VMEM((RING, 208, 128), BF16),
             pltpu.VMEM((RING, 208, 128), BF16),
             dma((32,)),
-            dma((30,)),
-            dma((32,)),
+            dma((60,)),
+            dma((64,)),
             dma((32,)),
             dma((32,)),
             dma((12,)),
@@ -573,7 +627,7 @@
         slim_floor_margin.reshape(1, -1),
         branch_content_tensor,
         emitted_switch_preact,
-        extra_log_fades.reshape(2, length // BLOCK, BLOCK),
+        jnp.swapaxes(extra_log_fades, 1, 2),
         channel_norm_scale.reshape(1, -1),
         emission_projection,
         mlp_norm_scale.reshape(1, -1),

time: 127 us -> 111 us (0.87); the launches traced: 125 us -> 110 us
  Pallas kernels: 121 us -> 108 us
    pallas_call x1, Pallas kernels: 121 us -> 108 us  [local(): pl.pallas_call(layer_kernel, out_shape=jax.ShapeDtypeStruct((rows, model)...]
where the time goes in v2:
time: 111 us; the launch traced here: 110 us
  Pallas kernels  108 us (97%)
  local copies, waits for them, and re-layouts  2.3 us (2%)
    pallas_call x1, Pallas kernels, local(): pl.pallas_call(layer_kernel, out_shape=jax.ShapeDtypeStruct((rows, model)...  108 us
    unnamed x1, local copies, waits for them, and re-layouts  2.3 us

profile of v2, /device:TPU:1, one launch (start us, length us, event | category | flops | bytes accessed | tf_op | source)
XLA Modules:
  0.0 109.9 jit_solution(3752034317565254913)
XLA Ops:
  0.0 107.6 %shard_map.154 = bf16[256,2048]{1,0:T(8,128)(2,1)} custom-call(bf16[256,2048]{1,0:T(8,128)(2,1)} %layer_source.1, bf16[1024,128]{1,0:T(8,128)(2,1)} %wide_query.1, bf16[1024,128]{1,0:T(8,128)(2,1)} %wide_forget.1, f32[1,128]{1,0:T(1,128)} %bitcast.13, bf16[64,1024]{1,0:T(8,128)(2,1)} %bitcast.9, bf16[64,1024]{1,0:T(8,128)(2,1)} %bitcast.10, ...), custom_call_target="tpu_custom_call" | custom-call | tf_op jit(solution)/shard_map/pallas_call | solution.py:579
  107.6 2.3 %copy.18 = bf16[256,2048]{1,0:T(8,128)(2,1)} copy(bf16[256,2048]{1,0:T(8,128)(2,1)} %shard_map.154) | data formatting | bytes 2097152

commit v3 on v2

--- a/solution.py
+++ b/solution.py
@@ -19,38 +19,13 @@
 TN = (((0,), (0,)), ((), ()))
 MESH = pl.DeviceIdType.MESH
 
-ARRIVALS = (
-    (3, 0, 0),
-    (1, 0, 1),
-    (0, 3, 0),
-    (0, 1, 1),
-    (3, 0, 1),
-    (1, 0, 0),
-    (0, 3, 1),
-    (0, 1, 0),
-    (2, 0, 0),
-    (2, 0, 1),
-    (3, 3, 0),
-    (3, 1, 1),
-    (1, 3, 0),
-    (1, 1, 1),
-    (3, 3, 1),
-    (3, 1, 0),
-    (0, 2, 0),
-    (0, 2, 1),
-    (1, 3, 1),
-    (1, 1, 0),
-    (2, 3, 0),
-    (2, 1, 1),
-    (2, 3, 1),
-    (2, 1, 0),
-    (3, 2, 0),
-    (3, 2, 1),
-    (1, 2, 0),
-    (1, 2, 1),
-    (2, 2, 0),
-    (2, 2, 1),
-)
+NEAR = ((3, 0, 0), (1, 0, 1), (0, 3, 0), (0, 1, 1), (3, 0, 1), (1, 0, 0))
+ACROSS = ((2, 0, 0), (2, 0, 1))
+CORNERS = ((3, 3, 0), (3, 1, 1), (1, 3, 0), (1, 1, 1), (2, 3, 0), (2, 1, 1))
+SIDES = ((0, 3, 1), (0, 1, 0))
+EDGES = ((3, 3, 1), (3, 1, 0), (0, 2, 0), (0, 2, 1), (1, 3, 1), (1, 1, 0))
+ENDS = ((2, 3, 1), (2, 1, 0), (3, 2, 0), (3, 2, 1))
+FAR = ((1, 2, 0), (1, 2, 1), (2, 2, 0), (2, 2, 1))
 
 
 def turn(value, step):
@@ -244,8 +219,8 @@
 
     handed = {}
 
-    def pump(part, first, last):
-        for i, j, h in ARRIVALS[first:last]:
+    def pump(part, arrivals):
+        for i, j, h in arrivals:
             arrived(shard(i, j, h, part, core), w_recv.at[mark(i, j, h, part)])
             if j == 0:
                 if (i, h) == (3, 0):
@@ -383,11 +358,8 @@
         )
         for group in groups
     )
-    pairs = length // (2 * BLOCK)
-    middle = lax.fori_loop(0, pairs // 2, advance, start, unroll=2)
-    pump(0, 0, 4)
     (wide_state, wide_log), (narrow_state, narrow_log) = lax.fori_loop(
-        pairs // 2, pairs, advance, middle, unroll=2
+        0, length // (2 * BLOCK), advance, start, unroll=2
     )
     packed = jnp.concatenate([narrow_state[0:64], narrow_state[64:128]], axis=1)
     narrow_log = jnp.concatenate([narrow_log, narrow_log], axis=1)
@@ -406,10 +378,11 @@
         for step in (1, 3, 2):
             send(src, src, s_send.at[base + step - 1], s_recv.at[base + here], {name: turn(here, step)})
         if base == 1:
+            pump(0, NEAR[0:4])
+        else:
+            pump(0, NEAR[4:6])
             x_relay(sources, 0)
-        else:
             start_weights(1)
-            pump(0, 4, 10)
         for step in (1, 3, 2):
             peer = turn(here, step)
             arrived(ref.at[peer], s_recv.at[base + peer])
@@ -437,11 +410,19 @@
     x_first(mixed, 8)
     x_second(mixed, 8)
 
-    pump(0, 10, 24)
+    pump(0, ACROSS + SIDES + CORNERS[0:2])
+    pump(1, NEAR)
+    pump(0, CORNERS[2:4] + EDGES + CORNERS[4:6])
+    pump(1, ACROSS)
     x_relay(mixed, 8)
     x_second(sources, 0)
-    pump(0, 24, 30)
-    pump(1, 0, 18)
+    pump(1, SIDES)
+    pump(0, ENDS[0:2])
+    pump(1, CORNERS[0:2])
+    pump(0, ENDS[2:4])
+    pump(1, CORNERS[2:4])
+    pump(0, FAR)
+    pump(1, EDGES + CORNERS[4:6])
     x_rest(mixed, 8)
     x_opposite(mixed, 8)
     x_opposite(sources, 0)
@@ -493,9 +474,9 @@
             hidden[:, pl.ds(pl.multiple_of(n * 128, 128), 128)] = found
             return carry
 
-        lax.fori_loop(0, ff // 128, widen, 0)
-
-    def shrink_all(out_ref, passed=False):
+        lax.fori_loop(0, ff // 128, widen, 0, unroll=4)
+
+    def shrink_all(out_ref, passed=False, first=0, last=model // 256):
         def shrink(n, carry):
             cols = pl.ds(pl.multiple_of(n * 256, 256), 256)
             four = weights[pl.ds(n * 4, 4), :, pl.ds(2 * ff, ff)].reshape(256, ff)
@@ -507,7 +488,7 @@
             out_ref[:, cols] = found.astype(out_ref.dtype)
             return carry
 
-        lax.fori_loop(0, model // 256, shrink, 0)
+        lax.fori_loop(first, last, shrink, 0, unroll=4)
 
     def send_sum(src, dst, k, step):
         send(src, dst, r_send.at[k], r_recv.at[k], {"tp": turn(x, step)})
@@ -515,31 +496,36 @@
     left_x, right_x = (turn(x, 3), turn(x, 1))
 
     emit(((turn(x, 2), 0), (turn(x, 2), 1)))
-    pump(1, 18, 30)
+    pump(1, ENDS)
     wait_partner(0)
     widen_all()
+    pump(1, FAR)
     wait_partner(1)
-    shrink_all(partial.at[0])
-    send_sum(partial.at[0, upper], passing.at[0], 0, 1)
-    send_sum(partial.at[0, lower], passing.at[1], 1, 3)
+    for k in range(2):
+        shrink_all(partial.at[0], first=k * (model // 512), last=(k + 1) * (model // 512))
+        cols = pl.ds(k * (model // 2), model // 2)
+        send_sum(partial.at[0, upper, cols], passing.at[0, :, cols], k, 1)
+        send_sum(partial.at[0, lower, cols], passing.at[1, :, cols], 2 + k, 3)
     emit(((right_x, 1), (left_x, 0)))
     widen_all()
     shrink_all(partial.at[1])
-    send_sum(partial.at[1, upper], landed.at[0, lower], 2, 1)
-    send_sum(partial.at[1, lower], landed.at[1, upper], 3, 3)
+    send_sum(partial.at[1, upper], landed.at[0, lower], 4, 1)
+    send_sum(partial.at[1, lower], landed.at[1, upper], 5, 3)
     x_rest(sources, 0)
     emit(((right_x, 0), (left_x, 1)))
     widen_all()
-    arrived(passing.at[0], r_recv.at[0])
-    arrived(passing.at[1], r_recv.at[1])
+    for k in range(2):
+        cols = pl.ds(k * (model // 2), model // 2)
+        arrived(passing.at[0, :, cols], r_recv.at[k])
+        arrived(passing.at[1, :, cols], r_recv.at[2 + k])
     shrink_all(partial.at[2], passed=True)
-    send_sum(partial.at[2, upper], landed.at[0, upper], 4, 1)
-    send_sum(partial.at[2, lower], landed.at[1, lower], 5, 3)
+    send_sum(partial.at[2, upper], landed.at[0, upper], 6, 1)
+    send_sum(partial.at[2, lower], landed.at[1, lower], 7, 3)
     emit(((x, 0), (x, 1)))
     widen_all()
     shrink_all(own_part)
     for n, (k, part) in enumerate(((0, lower), (1, upper), (0, upper), (1, lower))):
-        arrived(landed.at[k, part], r_recv.at[2 + n])
+        arrived(landed.at[k, part], r_recv.at[4 + n])
 
     def finish(n, carry):
         cols = pl.ds(pl.multiple_of(n * 256, 256), 256)
@@ -611,8 +597,8 @@
             dma((16,)),
             dma((9,)),
             dma((9,)),
-            dma((6,)),
-            dma((6,)),
+            dma((8,)),
+            dma((8,)),
         ],
         compiler_params=pltpu.CompilerParams(
             collective_id=0, has_side_effects=True, vmem_limit_bytes=62 * 1024 * 1024

time: 111 us -> 107 us (0.964)
  Pallas kernels: 108 us -> 104 us
    pallas_call x1, Pallas kernels: 108 us -> 104 us  [local(): pl.pallas_call(layer_kernel, out_shape=jax.ShapeDtypeStruct((rows, model)...]
where the time goes in v3:
time: 107 us
  Pallas kernels  104 us (97%)
  local copies, waits for them, and re-layouts  2.3 us (2%)
    pallas_call x1, Pallas kernels, local(): pl.pallas_call(layer_kernel, out_shape=jax.ShapeDtypeStruct((rows, model)...  104 us
    unnamed x1, local copies, waits for them, and re-layouts  2.3 us

profile of v3, /device:TPU:1, one launch (start us, length us, event | category | flops | bytes accessed | tf_op | source)
XLA Modules:
  0.0 106.7 jit_solution(13250933910457530825)
XLA Ops:
  0.0 104.3 %shard_map.154 = bf16[256,2048]{1,0:T(8,128)(2,1)} custom-call(bf16[256,2048]{1,0:T(8,128)(2,1)} %layer_source.1, bf16[1024,128]{1,0:T(8,128)(2,1)} %wide_query.1, bf16[1024,128]{1,0:T(8,128)(2,1)} %wide_forget.1, f32[1,128]{1,0:T(1,128)} %bitcast.13, bf16[64,1024]{1,0:T(8,128)(2,1)} %bitcast.9, bf16[64,1024]{1,0:T(8,128)(2,1)} %bitcast.10, ...), custom_call_target="tpu_custom_call" | custom-call | tf_op jit(solution)/shard_map/pallas_call | solution.py:565
  104.4 2.3 %copy.18 = bf16[256,2048]{1,0:T(8,128)(2,1)} copy(bf16[256,2048]{1,0:T(8,128)(2,1)} %shard_map.154) | data formatting | bytes 2097152

commit v4 on v3

--- a/solution.py
+++ b/solution.py
@@ -90,18 +90,18 @@
 
 def layer_kernel(
     layer_source,
-    wide_query,
-    wide_forget,
-    wide_gap,
-    narrow_query,
-    narrow_forget,
-    narrow_gap,
-    values,
-    switches,
-    fades,
-    channel_norm_scale,
+    wide_query_far,
+    wide_forget_far,
+    wide_gap_far,
+    narrow_query_far,
+    narrow_forget_far,
+    narrow_gap_far,
+    values_far,
+    switches_far,
+    fades_far,
+    channel_norm_scale_far,
     emission,
-    mlp_scale,
+    mlp_scale_far,
     gate_shard,
     up_shard,
     down_shard,
@@ -126,6 +126,18 @@
     core_states,
     y_states,
     z_states,
+    z_before,
+    wide_query,
+    wide_forget,
+    wide_gap,
+    narrow_query,
+    narrow_forget,
+    narrow_gap,
+    values,
+    switches,
+    fades,
+    channel_norm_scale,
+    mlp_scale,
     load_sem,
     w_send,
     w_recv,
@@ -133,6 +145,10 @@
     d_recv,
     x_send,
     x_recv,
+    m_send,
+    m_recv,
+    n_send,
+    n_recv,
     s_send,
     s_recv,
     r_send,
@@ -146,7 +162,7 @@
     depth = gate_shard.shape[0]
     sent = []
 
-    def send(src, dst, send_sem, recv_sem, to):
+    def send(src, dst, send_sem, recv_sem, to, alone=True):
         copy = pltpu.make_async_remote_copy(
             src_ref=src,
             dst_ref=dst,
@@ -156,7 +172,8 @@
             device_id_type=MESH,
         )
         copy.start()
-        sent.append(copy)
+        if alone:
+            sent.append(copy)
 
     partner = {"sp_2": other}
 
@@ -201,7 +218,7 @@
     def mark(i, j, h, part):
         return part * 32 + (i * 4 + j) * 2 + h
 
-    counts = {"w": 0, "x": 0}
+    counts = {"x": 0}
 
     def next_of(name):
         counts[name] += 1
@@ -210,12 +227,11 @@
     def forward(i, j, h, part, step, landing):
         src = shard(i, j, h, part, core)
         at = w_recv.at[mark(*landing, h, part)]
-        send(src, src, w_send.at[next_of("w")], at, toward(*step))
+        send(src, src, w_send.at[0], at, toward(*step), False)
 
     def hand_over(i, j, part):
         src = shard_part(i, j, part, core)
-        k = part * 16 + i * 4 + j
-        send(src, src, d_send.at[k], d_recv.at[k], partner)
+        send(src, src, d_send.at[0], d_recv.at[part], partner, False)
 
     handed = {}
 
@@ -247,9 +263,7 @@
         hand_over(0, 0, part)
 
     def wait_partner(part):
-        for i in range(RING):
-            for j in range(RING):
-                arrived(shard_part(i, j, part, other), d_recv.at[part * 16 + i * 4 + j])
+        arrived(weights.at[pl.ds(0, 16), :, columns_of[part]], d_recv.at[part])
 
     def x_piece(buffer, step, h):
         half = buffer.shape[1] // 2
@@ -265,10 +279,6 @@
     def x_first(buffer, base):
         x_forward(buffer, base, 0, 0, 1, 3)
         x_forward(buffer, base, 0, 1, 3, 1)
-
-    def x_second(buffer, base):
-        x_forward(buffer, base, 0, 1, 1, 3)
-        x_forward(buffer, base, 0, 0, 3, 1)
 
     def x_relay(buffer, base):
         x_wait(buffer, base, 3, 0)
@@ -280,28 +290,18 @@
         x_wait(buffer, base, 2, 0)
         x_wait(buffer, base, 2, 1)
 
-    def x_rest(buffer, base):
-        x_wait(buffer, base, 3, 1)
-        x_wait(buffer, base, 1, 0)
-
-    me = slot(0, 0, core)
-    loads = []
-
-    def load(src, dst):
-        copy = pltpu.make_async_copy(src, dst, load_sem.at[len(loads)])
-        copy.start()
-        loads.append(copy)
-
-    for n in range(ff // 128):
-        cols = pl.ds(n * 128, 128)
-        load(gate_shard.at[:, cols], weights.at[me, :, pl.ds(n * 256, 128)])
-        load(up_shard.at[:, cols], weights.at[me, :, pl.ds(n * 256 + 128, 128)])
-    load(down_shard, weights.at[me, :, pl.ds(2 * ff, ff)])
-    load(layer_source, sources.at[x])
-    first_loads = len(loads)
-    for t in range(RING):
-        for g in range(2):
-            load(emission.at[g, pl.ds(t * 128, 128), :], projection.at[t, pl.ds(g * 128, 128), :])
+    def head_piece(sender, r, h):
+        owner = turn(x, (sender + r) % RING)
+        at = owner * rows + (0 if h is None else h * (rows // 2))
+        count = rows if h is None else rows // 2
+        return mixed.at[turn(x, sender), pl.ds(pl.multiple_of(at, 128), count), :]
+
+    def heads_to(sender, r, h, k, step):
+        src = head_piece(sender, r, h)
+        send(src, src, m_send.at[k], m_recv.at[k], {"tp": turn(x, step)})
+
+    def heads_wait(sender, r, h, k):
+        arrived(head_piece(sender, r, h), m_recv.at[k])
 
     barrier = pltpu.get_barrier_semaphore()
     pl.semaphore_signal(barrier, inc=1, device_id=partner, device_id_type=MESH)
@@ -310,12 +310,53 @@
             pl.semaphore_signal(
                 barrier, inc=1, device_id={name: turn(here, step)}, device_id_type=MESH
             )
+
+    me = slot(0, 0, core)
+    loads = []
+
+    def load(src, dst, shared=None):
+        sem = load_sem.at[2 + len(loads) if shared is None else shared]
+        copy = pltpu.make_async_copy(src, dst, sem)
+        copy.start()
+        if shared is None:
+            loads.append(copy)
+
+    for n in range(ff // 128):
+        cols = pl.ds(n * 128, 128)
+        load(gate_shard.at[:, cols], weights.at[me, :, pl.ds(n * 256, 128)], 0)
+        load(up_shard.at[:, cols], weights.at[me, :, pl.ds(n * 256 + 128, 128)], 0)
+    load(down_shard, weights.at[me, :, pl.ds(2 * ff, ff)], 0)
+    load(layer_source, sources.at[x])
+    shard_loads = len(loads)
+    for src, dst in (
+        (wide_query_far, wide_query),
+        (wide_forget_far, wide_forget),
+        (wide_gap_far, wide_gap),
+        (narrow_query_far, narrow_query),
+        (narrow_forget_far, narrow_forget),
+        (narrow_gap_far, narrow_gap),
+        (values_far, values),
+        (fades_far, fades),
+    ):
+        load(src, dst)
+    first_loads = len(loads)
+    load(switches_far, switches)
+    load(channel_norm_scale_far, channel_norm_scale)
+    mixed_loads = len(loads)
+    load(mlp_scale_far, mlp_scale)
+    for t in range(RING):
+        for g in range(2):
+            load(emission.at[g, pl.ds(t * 128, 128), :], projection.at[t, pl.ds(g * 128, 128), :], 1)
+
     pl.semaphore_wait(barrier, 10)
 
-    for copy in loads[:first_loads]:
+    pltpu.make_async_copy(weights.at[me], weights.at[me], load_sem.at[0]).wait()
+    for copy in loads[:shard_loads]:
         copy.wait()
     start_weights(0)
     x_first(sources, 0)
+    for copy in loads[shard_loads:first_loads]:
+        copy.wait()
     for n in range(length // 128):
         cols = pl.ds(n * 128, 128)
         narrow_q[cols, :] = narrow_query[:, cols].astype(F32).T
@@ -372,29 +413,73 @@
     nothing = jax.tree.map(jnp.zeros_like, first)
     entering = selected(core == 1, first, nothing)
     total = combine(first, load_state(core_states, 1))
-    for base, ref, name, here in ((1, y_states, "sp_1", y), (5, z_states, "sp_0", z)):
-        store_state(ref, here, total)
-        src = ref.at[here]
-        for step in (1, 3, 2):
-            send(src, src, s_send.at[base + step - 1], s_recv.at[base + here], {name: turn(here, step)})
-        if base == 1:
-            pump(0, NEAR[0:4])
-        else:
-            pump(0, NEAR[4:6])
+    store_state(y_states, y, total)
+    src = y_states.at[y]
+    for step in (1, 3, 2):
+        send(src, src, s_send.at[step], s_recv.at[1 + y], {"sp_1": turn(y, step)})
+    pump(0, NEAR[0:4])
+    start_weights(1)
+    for step in (1, 3, 2):
+        if step == 2:
             x_relay(sources, 0)
-            start_weights(1)
-        for step in (1, 3, 2):
-            peer = turn(here, step)
-            arrived(ref.at[peer], s_recv.at[base + peer])
+        arrived(y_states.at[turn(y, step)], s_recv.at[1 + turn(y, step)])
+
+    def before(ref, here):
         inside, total = (nothing, nothing)
         for k in range(RING):
             total = combine(total, load_state(ref, k))
             inside = selected(k < here, total, inside)
-        entering = combine(inside, entering)
+        return (inside, total)
+
+    inside, total = before(y_states, y)
+    entering = combine(inside, entering)
+    src = z_states.at[z]
+    z_copies = [
+        pltpu.make_async_remote_copy(
+            src_ref=src,
+            dst_ref=src,
+            send_sem=s_send.at[3 + step],
+            recv_sem=s_recv.at[5 + z],
+            device_id={"sp_0": turn(z, step)},
+            device_id_type=MESH,
+        )
+        for step in (1, 3, 2)
+    ]
+    told = pltpu.make_async_remote_copy(
+        src_ref=z_before.at[0],
+        dst_ref=z_before.at[0],
+        send_sem=s_send.at[7],
+        recv_sem=s_recv.at[9],
+        device_id=partner,
+        device_id_type=MESH,
+    )
+
+    @pl.when(core == 1)
+    def _():
+        store_state(z_states, z, total)
+        for copy in z_copies:
+            copy.start()
+
+    pump(0, NEAR[4:6] + ACROSS + SIDES)
+
+    @pl.when(core == 1)
+    def _():
+        for step in (1, 3, 2):
+            arrived(z_states.at[turn(z, step)], s_recv.at[5 + turn(z, step)])
+        store_state(z_before, 0, before(z_states, z)[0])
+        told.start()
+
+    @pl.when(core == 0)
+    def _():
+        told.wait_recv()
+
+    entering = combine(load_state(z_before, 0), entering)
     _, _, wide_state, packed = entering
     narrow_state = jnp.concatenate([packed[:, 0:64], packed[:, 64:128]], axis=0).astype(BF16)
     wide_state = wide_state.astype(BF16)
 
+    for copy in loads[first_loads:mixed_loads]:
+        copy.wait()
     for n in range(RING):
         at = pl.ds(n * rows, rows)
         parts = []
@@ -407,32 +492,33 @@
             parts.append((out * jax.nn.silu(switches[g, at, :].astype(F32))).astype(BF16))
         mixed[x, at, :] = jnp.concatenate(parts, axis=1)
 
-    x_first(mixed, 8)
-    x_second(mixed, 8)
-
-    pump(0, ACROSS + SIDES + CORNERS[0:2])
-    pump(1, NEAR)
-    pump(0, CORNERS[2:4] + EDGES + CORNERS[4:6])
+    for k, (right, left) in enumerate((((2, 1), (2, 0)), ((0, 0), (0, 1)), ((1, None), (3, None)), ((3, None), (1, None)))):
+        heads_to(0, *right, k, 1)
+        heads_to(0, *left, 4 + k, 3)
+
+    pump(0, CORNERS[0:2])
+    pump(1, NEAR[0:4])
+    pump(0, CORNERS[2:4] + EDGES)
+    pump(1, NEAR[4:6])
+    for k, (right, left) in enumerate((((2, 1), (2, 0)), ((0, 0), (0, 1)))):
+        heads_wait(3, *right, k)
+        heads_to(3, *right, 8 + k, 1)
+        heads_wait(1, *left, 4 + k)
+        heads_to(1, *left, 11 + k, 3)
+    pump(0, CORNERS[4:6])
     pump(1, ACROSS)
-    x_relay(mixed, 8)
-    x_second(sources, 0)
-    pump(1, SIDES)
-    pump(0, ENDS[0:2])
-    pump(1, CORNERS[0:2])
-    pump(0, ENDS[2:4])
-    pump(1, CORNERS[2:4])
-    pump(0, FAR)
-    pump(1, EDGES + CORNERS[4:6])
-    x_rest(mixed, 8)
-    x_opposite(mixed, 8)
-    x_opposite(sources, 0)
-    for copy in loads[first_loads:]:
+    pltpu.make_async_copy(projection, projection, load_sem.at[1]).wait()
+    for copy in loads[mixed_loads:]:
         copy.wait()
+    heads_wait(3, 1, None, 2)
+    heads_wait(1, 3, None, 6)
+    heads_wait(2, 2, 1, 8)
+    heads_wait(2, 2, 0, 11)
 
     half = rows // 2
     upper, lower = (pl.ds(0, half), pl.ds(half, half))
 
-    def emit(pieces):
+    def emit(pieces, chunk, raw):
         def lines(owner, h):
             return pl.ds(pl.multiple_of(owner * rows + h * half, half), half)
 
@@ -449,7 +535,7 @@
             found = dot(left, projection[:, :, cols].reshape(4 * 256, 512))
             source = [sources[owner, pl.ds(h * half, half), cols] for owner, h in pieces]
             found = found + jnp.concatenate(source, axis=0).astype(F32)
-            updated[:, cols] = found
+            raw[:, cols] = found
             found = found * found
             return squares + (
                 (found[:, 0:128] + found[:, 128:256]) + (found[:, 256:384] + found[:, 384:512])
@@ -461,20 +547,20 @@
 
         def scale(n, carry):
             cols = pl.ds(pl.multiple_of(n * 512, 512), 512)
-            normed[:, cols] = (updated[:, cols] * inverse * mlp_scale[:, cols]).astype(BF16)
+            normed[chunk, :, cols] = (raw[:, cols] * inverse * mlp_scale[:, cols]).astype(BF16)
             return carry
 
         lax.fori_loop(0, model // 512, scale, 0)
 
-    def widen_all():
+    def widen_all(chunk, first=0, last=ff // 128):
         def widen(n, carry):
             cols = pl.ds(pl.multiple_of(n * 256, 256), 256)
-            both = dot(normed[...], weights[:, :, cols].reshape(model, 256))
+            both = dot(normed[chunk], weights[:, :, cols].reshape(model, 256))
             found = (jax.nn.silu(both[:, 0:128]) * both[:, 128:256]).astype(BF16)
             hidden[:, pl.ds(pl.multiple_of(n * 128, 128), 128)] = found
             return carry
 
-        lax.fori_loop(0, ff // 128, widen, 0, unroll=4)
+        lax.fori_loop(first, last, widen, 0, unroll=4)
 
     def shrink_all(out_ref, passed=False, first=0, last=model // 256):
         def shrink(n, carry):
@@ -495,25 +581,44 @@
 
     left_x, right_x = (turn(x, 3), turn(x, 1))
 
-    emit(((turn(x, 2), 0), (turn(x, 2), 1)))
-    pump(1, ENDS)
+    emit(((x, 0), (x, 1)), 3, updated)
+    send(normed.at[3, lower], normed.at[2, lower], n_send.at[0], n_recv.at[0], {"tp": right_x})
+    send(normed.at[3, upper], normed.at[2, upper], n_send.at[1], n_recv.at[1], {"tp": left_x})
+    heads_wait(3, 3, None, 3)
+    heads_to(3, 3, 1, 10, 1)
+    heads_wait(1, 1, None, 7)
+    heads_to(1, 1, 0, 13, 3)
+    pump(1, SIDES)
+    pump(0, ENDS[0:2])
+    pump(1, CORNERS[0:2])
+    pump(0, ENDS[2:4])
+    pump(1, CORNERS[2:4])
+    pump(0, FAR)
+    heads_wait(2, 0, 0, 9)
+    heads_wait(2, 0, 1, 12)
+    x_opposite(sources, 0)
+    emit(((turn(x, 2), 0), (turn(x, 2), 1)), 0, own_part)
+    pump(1, EDGES + CORNERS[4:6])
     wait_partner(0)
-    widen_all()
-    pump(1, FAR)
+    widen_all(0, 0, 8)
+    pump(1, ENDS + FAR)
+    widen_all(0, 8, ff // 128)
     wait_partner(1)
     for k in range(2):
         shrink_all(partial.at[0], first=k * (model // 512), last=(k + 1) * (model // 512))
         cols = pl.ds(k * (model // 2), model // 2)
         send_sum(partial.at[0, upper, cols], passing.at[0, :, cols], k, 1)
         send_sum(partial.at[0, lower, cols], passing.at[1, :, cols], 2 + k, 3)
-    emit(((right_x, 1), (left_x, 0)))
-    widen_all()
+    heads_wait(2, 3, 1, 10)
+    heads_wait(2, 1, 0, 13)
+    emit(((right_x, 1), (left_x, 0)), 1, own_part)
+    widen_all(1)
     shrink_all(partial.at[1])
     send_sum(partial.at[1, upper], landed.at[0, lower], 4, 1)
     send_sum(partial.at[1, lower], landed.at[1, upper], 5, 3)
-    x_rest(sources, 0)
-    emit(((right_x, 0), (left_x, 1)))
-    widen_all()
+    arrived(normed.at[2, lower], n_recv.at[0])
+    arrived(normed.at[2, upper], n_recv.at[1])
+    widen_all(2)
     for k in range(2):
         cols = pl.ds(k * (model // 2), model // 2)
         arrived(passing.at[0, :, cols], r_recv.at[k])
@@ -521,8 +626,7 @@
     shrink_all(partial.at[2], passed=True)
     send_sum(partial.at[2, upper], landed.at[0, upper], 6, 1)
     send_sum(partial.at[2, lower], landed.at[1, lower], 7, 3)
-    emit(((x, 0), (x, 1)))
-    widen_all()
+    widen_all(3)
     shrink_all(own_part)
     for n, (k, part) in enumerate(((0, lower), (1, upper), (0, upper), (1, lower))):
         arrived(landed.at[k, part], r_recv.at[4 + n])
@@ -536,6 +640,22 @@
     lax.fori_loop(0, model // 256, finish, 0)
     for copy in sent:
         copy.wait_send()
+    for count, sem in ((15, w_send), (16, d_send)):
+        shards = weights.at[pl.ds(0, count)]
+        pltpu.make_async_remote_copy(
+            src_ref=shards,
+            dst_ref=shards,
+            send_sem=sem.at[0],
+            recv_sem=sem.at[0],
+            device_id=partner,
+            device_id_type=MESH,
+        ).wait_send()
+
+    @pl.when(core == 1)
+    def _():
+        for copy in z_copies:
+            copy.wait_send()
+        told.wait_send()
 
 
 def local(
@@ -564,8 +684,8 @@
     dma = pltpu.SemaphoreType.DMA
     return pl.pallas_call(
         layer_kernel,
-        out_shape=jax.ShapeDtypeStruct((rows, model), BF16),
-        in_specs=[far] + [vmem] * 10 + [far, vmem, far, far, far],
+        out_shape=pltpu.VMEM((rows, model), BF16),
+        in_specs=[far] * 16,
         out_specs=vmem,
         scratch_shapes=[
             pltpu.VMEM((32, depth, 3 * ff), BF16),
@@ -573,7 +693,7 @@
             pltpu.VMEM((RING, length, 256), BF16),
             pltpu.VMEM((RING, 256, model), BF16),
             pltpu.VMEM((rows, model), F32),
-            pltpu.VMEM((rows, model), BF16),
+            pltpu.VMEM((RING, rows, model), BF16),
             pltpu.VMEM((rows, ff), BF16),
             pltpu.VMEM((3, rows, model), BF16),
             pltpu.VMEM((rows, model), F32),
@@ -588,15 +708,31 @@
             pltpu.VMEM((2, 208, 128), BF16),
             pltpu.VMEM((RING, 208, 128), BF16),
             pltpu.VMEM((RING, 208, 128), BF16),
-            dma((32,)),
-            dma((60,)),
+            pltpu.VMEM((1, 208, 128), BF16),
+            pltpu.VMEM((length, 128), BF16),
+            pltpu.VMEM((length, 128), BF16),
+            pltpu.VMEM((1, 128), F32),
+            pltpu.VMEM((64, length), BF16),
+            pltpu.VMEM((64, length), BF16),
+            pltpu.VMEM((1, 64), F32),
+            pltpu.VMEM((2, length, 128), BF16),
+            pltpu.VMEM((2, length, 128), BF16),
+            pltpu.VMEM((2, 1, length), F32),
+            pltpu.VMEM((1, 128), F32),
+            pltpu.VMEM((1, model), F32),
+            dma((14,)),
+            dma((1,)),
             dma((64,)),
-            dma((32,)),
-            dma((32,)),
-            dma((12,)),
-            dma((16,)),
-            dma((9,)),
-            dma((9,)),
+            dma((1,)),
+            dma((2,)),
+            dma((4,)),
+            dma((8,)),
+            dma((14,)),
+            dma((14,)),
+            dma((2,)),
+            dma((2,)),
+            dma((8,)),
+            dma((10,)),
             dma((8,)),
             dma((8,)),
         ],

time: 107 us -> 98 us (0.916)
  Pallas kernels: 104 us -> 96.9 us
  local copies, waits for them, and re-layouts: 2.3 us -> 0.97 us
    pallas_call x1, Pallas kernels: 104 us -> 96.9 us  [local(): pl.pallas_call(layer_kernel, out_shape=pltpu.VMEM((rows, model), BF16), i...]
    unnamed x1, local copies, waits for them, and re-layouts: 2.3 us -> 0.97 us
where the time goes in v4:
time: 98 us; the launch traced here: 97.9 us
  Pallas kernels  96.9 us (99%)
    pallas_call x1, Pallas kernels, local(): pl.pallas_call(layer_kernel, out_shape=pltpu.VMEM((rows, model), BF16), i...  96.9 us

profile of v4, /device:TPU:1, one launch (start us, length us, event | category | flops | bytes accessed | tf_op | source)
XLA Modules:
  0.0 97.9 jit_solution(1322399326661297206)
XLA Ops:
  0.0 96.9 %shard_map.154 = bf16[256,2048]{1,0:T(8,128)(2,1)S(1)} custom-call(bf16[256,2048]{1,0:T(8,128)(2,1)} %layer_source.1, bf16[1024,128]{1,0:T(8,128)(2,1)} %wide_query_far.1, bf16[1024,128]{1,0:T(8,128)(2,1)} %wide_forget_far.1, f32[1,128]{1,0:T(1,128)} %bitcast.13, bf16[64,1024]{1,0:T(8,128)(2,1)} %bitcast.9, bf16[64,1024]{1,0:T(8,128)(2,1)} %bitcast.10, ...), custom_call_target="tpu_custom_call" | custom-call | tf_op jit(solution)/shard_map/pallas_call | solution.py:685
  96.9 1.0 copy.18

commit v5 on v4

--- a/solution.py
+++ b/solution.py
@@ -26,6 +26,10 @@
 EDGES = ((3, 3, 1), (3, 1, 0), (0, 2, 0), (0, 2, 1), (1, 3, 1), (1, 1, 0))
 ENDS = ((2, 3, 1), (2, 1, 0), (3, 2, 0), (3, 2, 1))
 FAR = ((1, 2, 0), (1, 2, 1), (2, 2, 0), (2, 2, 1))
+
+
+PASSED = NEAR + ACROSS + CORNERS
+GROUPS = (SIDES, EDGES, ENDS, FAR)
 
 
 def turn(value, step):
@@ -216,13 +220,9 @@
         return {"sp_0": at_z, "sp_1": at_y}
 
     def mark(i, j, h, part):
-        return part * 32 + (i * 4 + j) * 2 + h
-
-    counts = {"x": 0}
-
-    def next_of(name):
-        counts[name] += 1
-        return counts[name] - 1
+        if (i, j, h) in PASSED:
+            return part * 18 + PASSED.index((i, j, h))
+        return part * 18 + 14 + [(i, j, h) in group for group in GROUPS].index(True)
 
     def forward(i, j, h, part, step, landing):
         src = shard(i, j, h, part, core)
@@ -232,6 +232,12 @@
     def hand_over(i, j, part):
         src = shard_part(i, j, part, core)
         send(src, src, d_send.at[0], d_recv.at[part], partner, False)
+
+    def spread(i, h, part, passed_on):
+        if (h == 0) == passed_on:
+            forward(i, 0, h, part, (0, 1), (i, 3))
+        else:
+            forward(i, 0, h, part, (0, 3), (i, 1))
 
     handed = {}
 
@@ -243,16 +249,26 @@
                     forward(i, 0, h, part, (1, 0), (2, 0))
                 if (i, h) == (1, 1):
                     forward(i, 0, h, part, (3, 0), (2, 0))
-                forward(i, 0, h, part, (0, 1), (i, 3))
-                forward(i, 0, h, part, (0, 3), (i, 1))
+                spread(i, h, part, True)
+                if part == 0:
+                    spread(i, h, part, False)
             else:
                 if (j, h) == (3, 0):
                     forward(i, j, h, part, (0, 1), (i, 2))
                 if (j, h) == (1, 1):
                     forward(i, j, h, part, (0, 3), (i, 2))
-            handed[(i, j, part)] = handed.get((i, j, part), 0) + 1
-            if handed[(i, j, part)] == 2:
-                hand_over(i, j, part)
+            seen(i, j, part)
+
+    def seen(i, j, part):
+        handed[(i, j, part)] = handed.get((i, j, part), 0) + 1
+        if handed[(i, j, part)] == 2:
+            hand_over(i, j, part)
+
+    def pump_group(part, group):
+        halves = weights.at[pl.ds(0, len(group) // 2), :, columns_of[part]]
+        arrived(halves, w_recv.at[mark(*group[0], part)])
+        for i, j, _ in group:
+            seen(i, j, part)
 
     def start_weights(part):
         for h in range(2):
@@ -265,30 +281,28 @@
     def wait_partner(part):
         arrived(weights.at[pl.ds(0, 16), :, columns_of[part]], d_recv.at[part])
 
-    def x_piece(buffer, step, h):
-        half = buffer.shape[1] // 2
-        return buffer.at[turn(x, step), pl.ds(h * half, half), :]
-
-    def x_forward(buffer, base, step, h, to, landing):
-        src = x_piece(buffer, step, h)
-        send(src, src, x_send.at[next_of("x")], x_recv.at[base + landing * 2 + h], {"tp": turn(x, to)})
-
-    def x_wait(buffer, base, step, h):
-        arrived(x_piece(buffer, step, h), x_recv.at[base + step * 2 + h])
-
-    def x_first(buffer, base):
-        x_forward(buffer, base, 0, 0, 1, 3)
-        x_forward(buffer, base, 0, 1, 3, 1)
-
-    def x_relay(buffer, base):
-        x_wait(buffer, base, 3, 0)
-        x_forward(buffer, base, 3, 0, 1, 2)
-        x_wait(buffer, base, 1, 1)
-        x_forward(buffer, base, 1, 1, 3, 2)
-
-    def x_opposite(buffer, base):
-        x_wait(buffer, base, 2, 0)
-        x_wait(buffer, base, 2, 1)
+    def rows_piece(step, q):
+        quarter = rows // 4
+        return sources.at[turn(x, step), pl.ds(q * quarter, quarter), :]
+
+    def rows_to(step, q, landing, to):
+        src = rows_piece(step, q)
+        at = x_recv.at[min(landing, 4)]
+        send(src, src, x_send.at[0], at, {"tp": turn(x, to)}, False)
+
+    def rows_start():
+        for k in range(2):
+            rows_to(0, k, k, 1)
+            rows_to(0, 2 + k, 2 + k, 3)
+
+    def rows_relay(k):
+        arrived(rows_piece(3, k), x_recv.at[k])
+        rows_to(3, k, 4 + k, 1)
+        arrived(rows_piece(1, 2 + k), x_recv.at[2 + k])
+        rows_to(1, 2 + k, 6 + k, 3)
+
+    def rows_opposite():
+        arrived(sources.at[turn(x, 2)], x_recv.at[4])
 
     def head_piece(sender, r, h):
         owner = turn(x, (sender + r) % RING)
@@ -298,7 +312,10 @@
 
     def heads_to(sender, r, h, k, step):
         src = head_piece(sender, r, h)
-        send(src, src, m_send.at[k], m_recv.at[k], {"tp": turn(x, step)})
+        send(src, src, m_send.at[0], m_recv.at[k], {"tp": turn(x, step)}, False)
+
+    def heads_wait_all(count, k):
+        arrived(mixed.at[0, pl.ds(0, count), :], m_recv.at[k])
 
     def heads_wait(sender, r, h, k):
         arrived(head_piece(sender, r, h), m_recv.at[k])
@@ -354,7 +371,7 @@
     for copy in loads[:shard_loads]:
         copy.wait()
     start_weights(0)
-    x_first(sources, 0)
+    rows_start()
     for copy in loads[shard_loads:first_loads]:
         copy.wait()
     for n in range(length // 128):
@@ -419,9 +436,10 @@
         send(src, src, s_send.at[step], s_recv.at[1 + y], {"sp_1": turn(y, step)})
     pump(0, NEAR[0:4])
     start_weights(1)
+    rows_relay(0)
     for step in (1, 3, 2):
         if step == 2:
-            x_relay(sources, 0)
+            rows_relay(1)
         arrived(y_states.at[turn(y, step)], s_recv.at[1 + turn(y, step)])
 
     def before(ref, here):
@@ -460,7 +478,8 @@
         for copy in z_copies:
             copy.start()
 
-    pump(0, NEAR[4:6] + ACROSS + SIDES)
+    pump(0, NEAR[4:6] + ACROSS)
+    pump_group(0, SIDES)
 
     @pl.when(core == 1)
     def _():
@@ -492,28 +511,39 @@
             parts.append((out * jax.nn.silu(switches[g, at, :].astype(F32))).astype(BF16))
         mixed[x, at, :] = jnp.concatenate(parts, axis=1)
 
-    for k, (right, left) in enumerate((((2, 1), (2, 0)), ((0, 0), (0, 1)), ((1, None), (3, None)), ((3, None), (1, None)))):
-        heads_to(0, *right, k, 1)
-        heads_to(0, *left, 4 + k, 3)
+    own_half, across_half = (((2, 1), (2, 0)), ((0, 0), (0, 1)))
+    own_rows, across_rows = (((1, None), (3, None)), ((3, None), (1, None)))
+    for (right, left), to_right, to_left in (
+        (own_half, 3, 4),
+        (own_rows, 0, 0),
+        (across_half, 5, 6),
+        (across_rows, 7, 8),
+    ):
+        heads_to(0, *right, to_right, 1)
+        heads_to(0, *left, to_left, 3)
+
+    def heads_relay(k, landing, right, left):
+        heads_wait(3, *right, k)
+        heads_to(3, *right, landing, 1)
+        heads_wait(1, *left, k + 1)
+        heads_to(1, *left, landing, 3)
 
     pump(0, CORNERS[0:2])
     pump(1, NEAR[0:4])
-    pump(0, CORNERS[2:4] + EDGES)
+    heads_relay(3, 0, *own_half)
+    pump(0, CORNERS[2:4])
+    pump_group(0, EDGES)
     pump(1, NEAR[4:6])
-    for k, (right, left) in enumerate((((2, 1), (2, 0)), ((0, 0), (0, 1)))):
-        heads_wait(3, *right, k)
-        heads_to(3, *right, 8 + k, 1)
-        heads_wait(1, *left, 4 + k)
-        heads_to(1, *left, 11 + k, 3)
     pump(0, CORNERS[4:6])
     pump(1, ACROSS)
+    for i in (3, 1, 2):
+        for h in range(2):
+            spread(i, h, 1, False)
+    heads_relay(5, 1, *across_half)
     pltpu.make_async_copy(projection, projection, load_sem.at[1]).wait()
     for copy in loads[mixed_loads:]:
         copy.wait()
-    heads_wait(3, 1, None, 2)
-    heads_wait(1, 3, None, 6)
-    heads_wait(2, 2, 1, 8)
-    heads_wait(2, 2, 0, 11)
+    heads_wait_all(768, 0)
 
     half = rows // 2
     upper, lower = (pl.ds(0, half), pl.ds(half, half))
@@ -577,71 +607,84 @@
         lax.fori_loop(first, last, shrink, 0, unroll=4)
 
     def send_sum(src, dst, k, step):
-        send(src, dst, r_send.at[k], r_recv.at[k], {"tp": turn(x, step)})
+        send(src, dst, r_send.at[0], r_recv.at[k], {"tp": turn(x, step)}, False)
 
     left_x, right_x = (turn(x, 3), turn(x, 1))
 
     emit(((x, 0), (x, 1)), 3, updated)
-    send(normed.at[3, lower], normed.at[2, lower], n_send.at[0], n_recv.at[0], {"tp": right_x})
-    send(normed.at[3, upper], normed.at[2, upper], n_send.at[1], n_recv.at[1], {"tp": left_x})
-    heads_wait(3, 3, None, 3)
-    heads_to(3, 3, 1, 10, 1)
-    heads_wait(1, 1, None, 7)
-    heads_to(1, 1, 0, 13, 3)
-    pump(1, SIDES)
-    pump(0, ENDS[0:2])
+    send(normed.at[3, lower], normed.at[2, lower], n_send.at[0], n_recv.at[0], {"tp": right_x}, False)
+    send(normed.at[3, upper], normed.at[2, upper], n_send.at[0], n_recv.at[0], {"tp": left_x}, False)
+    heads_wait(3, 3, None, 7)
+    heads_to(3, 3, 1, 2, 1)
+    heads_wait(1, 1, None, 8)
+    heads_to(1, 1, 0, 2, 3)
+    pump_group(1, SIDES)
     pump(1, CORNERS[0:2])
-    pump(0, ENDS[2:4])
+    heads_wait_all(256, 1)
+    rows_opposite()
+    emit(((turn(x, 2), 0), (turn(x, 2), 1)), 0, own_part)
     pump(1, CORNERS[2:4])
-    pump(0, FAR)
-    heads_wait(2, 0, 0, 9)
-    heads_wait(2, 0, 1, 12)
-    x_opposite(sources, 0)
-    emit(((turn(x, 2), 0), (turn(x, 2), 1)), 0, own_part)
-    pump(1, EDGES + CORNERS[4:6])
+    pump_group(0, ENDS)
+    pump(1, CORNERS[4:6])
+    pump_group(0, FAR)
+    pump_group(1, EDGES)
     wait_partner(0)
     widen_all(0, 0, 8)
-    pump(1, ENDS + FAR)
+    pump_group(1, ENDS)
+    pump_group(1, FAR)
     widen_all(0, 8, ff // 128)
     wait_partner(1)
     for k in range(2):
         shrink_all(partial.at[0], first=k * (model // 512), last=(k + 1) * (model // 512))
         cols = pl.ds(k * (model // 2), model // 2)
-        send_sum(partial.at[0, upper, cols], passing.at[0, :, cols], k, 1)
-        send_sum(partial.at[0, lower, cols], passing.at[1, :, cols], 2 + k, 3)
-    heads_wait(2, 3, 1, 10)
-    heads_wait(2, 1, 0, 13)
+        send_sum(partial.at[0, upper, cols], passing.at[0, :, cols], 0, 1)
+        send_sum(partial.at[0, lower, cols], passing.at[1, :, cols], 0, 3)
+    heads_wait_all(256, 2)
     emit(((right_x, 1), (left_x, 0)), 1, own_part)
     widen_all(1)
     shrink_all(partial.at[1])
-    send_sum(partial.at[1, upper], landed.at[0, lower], 4, 1)
-    send_sum(partial.at[1, lower], landed.at[1, upper], 5, 3)
-    arrived(normed.at[2, lower], n_recv.at[0])
-    arrived(normed.at[2, upper], n_recv.at[1])
+    send_sum(partial.at[1, upper], landed.at[0, lower], 1, 1)
+    send_sum(partial.at[1, lower], landed.at[1, upper], 1, 3)
+    arrived(normed.at[2], n_recv.at[0])
     widen_all(2)
+    arrived(passing, r_recv.at[0])
+    shrink_all(partial.at[2], passed=True)
     for k in range(2):
         cols = pl.ds(k * (model // 2), model // 2)
-        arrived(passing.at[0, :, cols], r_recv.at[k])
-        arrived(passing.at[1, :, cols], r_recv.at[2 + k])
-    shrink_all(partial.at[2], passed=True)
-    send_sum(partial.at[2, upper], landed.at[0, upper], 6, 1)
-    send_sum(partial.at[2, lower], landed.at[1, lower], 7, 3)
+        send_sum(partial.at[2, upper, cols], landed.at[0, upper, cols], 2 + k, 1)
+        send_sum(partial.at[2, lower, cols], landed.at[1, lower, cols], 2 + k, 3)
     widen_all(3)
     shrink_all(own_part)
-    for n, (k, part) in enumerate(((0, lower), (1, upper), (0, upper), (1, lower))):
-        arrived(landed.at[k, part], r_recv.at[4 + n])
+    arrived(landed.at[0], r_recv.at[1])
+
+    def gather_early(n, carry):
+        cols = pl.ds(pl.multiple_of(n * 256, 256), 256)
+        early = jnp.concatenate([landed[1, upper, cols], landed[0, lower, cols]], axis=0)
+        summed = own_part[:, cols] + early.astype(F32)
+        updated[:, cols] = updated[:, cols] + 0.5 * summed
+        return carry
+
+    lax.fori_loop(0, model // 256, gather_early, 0)
 
     def finish(n, carry):
         cols = pl.ds(pl.multiple_of(n * 256, 256), 256)
-        summed = own_part[:, cols] + (landed[0, :, cols].astype(F32) + landed[1, :, cols].astype(F32))
-        layer_out[:, cols] = (updated[:, cols] + 0.5 * summed).astype(BF16)
+        late = jnp.concatenate([landed[0, upper, cols], landed[1, lower, cols]], axis=0)
+        layer_out[:, cols] = (updated[:, cols] + 0.5 * late.astype(F32)).astype(BF16)
         return carry
 
-    lax.fori_loop(0, model // 256, finish, 0)
+    for k in range(2):
+        arrived(landed.at[0, :, pl.ds(0, model // 2)], r_recv.at[2 + k])
+        lax.fori_loop(k * (model // 512), (k + 1) * (model // 512), finish, 0, unroll=2)
     for copy in sent:
         copy.wait_send()
-    for count, sem in ((15, w_send), (16, d_send)):
-        shards = weights.at[pl.ds(0, count)]
+    for shards, sem in (
+        (weights.at[pl.ds(0, 15)], w_send),
+        (weights.at[pl.ds(0, 16)], d_send),
+        (sources.at[pl.ds(0, 2)], x_send),
+        (mixed.at[pl.ds(0, 3), pl.ds(0, 3 * rows), :], m_send),
+        (normed.at[0], n_send),
+        (partial, r_send),
+    ):
         pltpu.make_async_remote_copy(
             src_ref=shards,
             dst_ref=shards,
@@ -722,19 +765,19 @@
             pltpu.VMEM((1, model), F32),
             dma((14,)),
             dma((1,)),
-            dma((64,)),
+            dma((36,)),
             dma((1,)),
             dma((2,)),
-            dma((4,)),
-            dma((8,)),
-            dma((14,)),
-            dma((14,)),
-            dma((2,)),
-            dma((2,)),
+            dma((1,)),
+            dma((5,)),
+            dma((1,)),
+            dma((9,)),
+            dma((1,)),
+            dma((1,)),
             dma((8,)),
             dma((10,)),
-            dma((8,)),
-            dma((8,)),
+            dma((1,)),
+            dma((4,)),
         ],
         compiler_params=pltpu.CompilerParams(
             collective_id=0, has_side_effects=True, vmem_limit_bytes=62 * 1024 * 1024

time: 98 us -> 97.2 us (level)
  no operation moved by 1% of the time
where the time goes in v5:
time: 97.2 us; the launch traced here: 97.1 us
  Pallas kernels  96.1 us (99%)
    pallas_call x1, Pallas kernels, local(): pl.pallas_call(layer_kernel, out_shape=pltpu.VMEM((rows, model), BF16), i...  96.1 us

profile of v5, /device:TPU:1, one launch (start us, length us, event | category | flops | bytes accessed | tf_op | source)
XLA Modules:
  0.0 97.1 jit_solution(4242672726843592709)
XLA Ops:
  0.0 96.1 %shard_map.154 = bf16[256,2048]{1,0:T(8,128)(2,1)S(1)} custom-call(bf16[256,2048]{1,0:T(8,128)(2,1)} %layer_source.1, bf16[1024,128]{1,0:T(8,128)(2,1)} %wide_query_far.1, bf16[1024,128]{1,0:T(8,128)(2,1)} %wide_forget_far.1, f32[1,128]{1,0:T(1,128)} %bitcast.13, bf16[64,1024]{1,0:T(8,128)(2,1)} %bitcast.9, bf16[64,1024]{1,0:T(8,128)(2,1)} %bitcast.10, ...), custom_call_target="tpu_custom_call" | custom-call | tf_op jit(solution)/shard_map/pallas_call | solution.py:728
  96.2 1.0 %copy.18 = bf16[256,2048]{1,0:T(8,128)(2,1)} copy(bf16[256,2048]{1,0:T(8,128)(2,1)S(1)} %shard_map.154) | data formatting | bytes 2097152

commit v6 on v5

--- a/solution.py
+++ b/solution.py
@@ -231,7 +231,10 @@
 
     def hand_over(i, j, part):
         src = shard_part(i, j, part, core)
-        send(src, src, d_send.at[0], d_recv.at[part], partner, False)
+        landing = part
+        if part == 1:
+            landing = jnp.where(core == 0, 1 if j in (0, 3) else 2, 1 if i in (0, 3) else 2)
+        send(src, src, d_send.at[0], d_recv.at[landing], partner, False)
 
     def spread(i, h, part, passed_on):
         if (h == 0) == passed_on:
@@ -280,6 +283,9 @@
 
     def wait_partner(part):
         arrived(weights.at[pl.ds(0, 16), :, columns_of[part]], d_recv.at[part])
+
+    def wait_partner_half(near):
+        arrived(weights.at[pl.ds(0, 8), :, columns_of[1]], d_recv.at[1 if near else 2])
 
     def rows_piece(step, q):
         quarter = rows // 4
@@ -592,19 +598,22 @@
 
         lax.fori_loop(first, last, widen, 0, unroll=4)
 
-    def shrink_all(out_ref, passed=False, first=0, last=model // 256):
+    def shrink_tile(out_ref, n, passed=False):
+        cols = pl.ds(pl.multiple_of(n * 256, 256), 256)
+        four = weights[pl.ds(n * 4, 4), :, pl.ds(2 * ff, ff)].reshape(256, ff)
+        found = dot(hidden[...], four, NT)
+        if passed:
+            found = found + jnp.concatenate(
+                [passing[0, :, cols], passing[1, :, cols]], axis=0
+            ).astype(F32)
+        out_ref[:, cols] = found.astype(out_ref.dtype)
+
+    def shrink_all(out_ref, passed=False):
         def shrink(n, carry):
-            cols = pl.ds(pl.multiple_of(n * 256, 256), 256)
-            four = weights[pl.ds(n * 4, 4), :, pl.ds(2 * ff, ff)].reshape(256, ff)
-            found = dot(hidden[...], four, NT)
-            if passed:
-                found = found + jnp.concatenate(
-                    [passing[0, :, cols], passing[1, :, cols]], axis=0
-                ).astype(F32)
-            out_ref[:, cols] = found.astype(out_ref.dtype)
+            shrink_tile(out_ref, n, passed)
             return carry
 
-        lax.fori_loop(first, last, shrink, 0, unroll=4)
+        lax.fori_loop(0, model // 256, shrink, 0, unroll=4)
 
     def send_sum(src, dst, k, step):
         send(src, dst, r_send.at[0], r_recv.at[k], {"tp": turn(x, step)}, False)
@@ -625,20 +634,26 @@
     emit(((turn(x, 2), 0), (turn(x, 2), 1)), 0, own_part)
     pump(1, CORNERS[2:4])
     pump_group(0, ENDS)
-    pump(1, CORNERS[4:6])
     pump_group(0, FAR)
+    pump(1, CORNERS[4:5])
+    wait_partner(0)
+    widen_all(0, 0, 4)
+    pump(1, CORNERS[5:6])
     pump_group(1, EDGES)
-    wait_partner(0)
-    widen_all(0, 0, 8)
+    widen_all(0, 4, 8)
     pump_group(1, ENDS)
-    pump_group(1, FAR)
     widen_all(0, 8, ff // 128)
-    wait_partner(1)
-    for k in range(2):
-        shrink_all(partial.at[0], first=k * (model // 512), last=(k + 1) * (model // 512))
-        cols = pl.ds(k * (model // 2), model // 2)
-        send_sum(partial.at[0, upper, cols], passing.at[0, :, cols], 0, 1)
-        send_sum(partial.at[0, lower, cols], passing.at[1, :, cols], 0, 3)
+    for near, steps in ((True, (0, 3)), (False, (1, 2))):
+        if not near:
+            pump_group(1, FAR)
+        wait_partner_half(near)
+        for step in steps:
+            for n in range(2):
+                shrink_tile(partial.at[0], turn(z, step) * 2 + n)
+        for step in steps:
+            cols = pl.ds(pl.multiple_of(turn(z, step) * 512, 512), 512)
+            send_sum(partial.at[0, upper, cols], passing.at[0, :, cols], 0, 1)
+            send_sum(partial.at[0, lower, cols], passing.at[1, :, cols], 0, 3)
     heads_wait_all(256, 2)
     emit(((right_x, 1), (left_x, 0)), 1, own_part)
     widen_all(1)
@@ -767,7 +782,7 @@
             dma((1,)),
             dma((36,)),
             dma((1,)),
-            dma((2,)),
+            dma((3,)),
             dma((1,)),
             dma((5,)),
             dma((1,)),

time: 97.2 us -> 95.6 us (0.984)
  Pallas kernels: 96.1 us -> 94.5 us
    pallas_call x1, Pallas kernels: 96.1 us -> 94.5 us  [local(): pl.pallas_call(layer_kernel, out_shape=pltpu.VMEM((rows, model), BF16), i...]
where the time goes in v6:
time: 95.6 us; the launch traced here: 95.5 us
  Pallas kernels  94.5 us (99%)
  local copies, waits for them, and re-layouts  0.97 us (1%)
    pallas_call x1, Pallas kernels, local(): pl.pallas_call(layer_kernel, out_shape=pltpu.VMEM((rows, model), BF16), i...  94.5 us

profile of v6, /device:TPU:1, one launch (start us, length us, event | category | flops | bytes accessed | tf_op | source)
XLA Modules:
  0.0 95.5 jit_solution(10544193482493869103)
XLA Ops:
  0.0 94.5 %shard_map.154 = bf16[256,2048]{1,0:T(8,128)(2,1)S(1)} custom-call(bf16[256,2048]{1,0:T(8,128)(2,1)} %layer_source.1, bf16[1024,128]{1,0:T(8,128)(2,1)} %wide_query_far.1, bf16[1024,128]{1,0:T(8,128)(2,1)} %wide_forget_far.1, f32[1,128]{1,0:T(1,128)} %bitcast.13, bf16[64,1024]{1,0:T(8,128)(2,1)} %bitcast.9, bf16[64,1024]{1,0:T(8,128)(2,1)} %bitcast.10, ...), custom_call_target="tpu_custom_call" | custom-call | tf_op jit(solution)/shard_map/pallas_call | solution.py:743
  94.5 1.0 %copy.18 = bf16[256,2048]{1,0:T(8,128)(2,1)} copy(bf16[256,2048]{1,0:T(8,128)(2,1)S(1)} %shard_map.154) | data formatting | bytes 2097152

commit v7 on v6

--- a/solution.py
+++ b/solution.py
@@ -377,6 +377,7 @@
     for copy in loads[:shard_loads]:
         copy.wait()
     start_weights(0)
+    start_weights(1)
     rows_start()
     for copy in loads[shard_loads:first_loads]:
         copy.wait()
@@ -441,7 +442,6 @@
     for step in (1, 3, 2):
         send(src, src, s_send.at[step], s_recv.at[1 + y], {"sp_1": turn(y, step)})
     pump(0, NEAR[0:4])
-    start_weights(1)
     rows_relay(0)
     for step in (1, 3, 2):
         if step == 2:

time: 95.6 us -> 94.1 us (0.984)
  Pallas kernels: 94.5 us -> 93 us
    pallas_call x1, Pallas kernels: 94.5 us -> 93 us  [local(): pl.pallas_call(layer_kernel, out_shape=pltpu.VMEM((rows, model), BF16), i...]
where the time goes in v7:
time: 94.1 us; the launch traced here: 94 us
  Pallas kernels  93 us (99%)
  local copies, waits for them, and re-layouts  0.97 us (1%)
    pallas_call x1, Pallas kernels, local(): pl.pallas_call(layer_kernel, out_shape=pltpu.VMEM((rows, model), BF16), i...  93 us

profile of v7, /device:TPU:1, one launch (start us, length us, event | category | flops | bytes accessed | tf_op | source)
XLA Modules:
  0.0 94.0 jit_solution(4933235074682024186)
XLA Ops:
  0.0 93.0 %shard_map.154 = bf16[256,2048]{1,0:T(8,128)(2,1)S(1)} custom-call(bf16[256,2048]{1,0:T(8,128)(2,1)} %layer_source.1, bf16[1024,128]{1,0:T(8,128)(2,1)} %wide_query_far.1, bf16[1024,128]{1,0:T(8,128)(2,1)} %wide_forget_far.1, f32[1,128]{1,0:T(1,128)} %bitcast.13, bf16[64,1024]{1,0:T(8,128)(2,1)} %bitcast.9, bf16[64,1024]{1,0:T(8,128)(2,1)} %bitcast.10, ...), custom_call_target="tpu_custom_call" | custom-call | tf_op jit(solution)/shard_map/pallas_call | solution.py:743
  93.0 1.0 %copy.18 = bf16[256,2048]{1,0:T(8,128)(2,1)} copy(bf16[256,2048]{1,0:T(8,128)(2,1)S(1)} %shard_map.154) | data formatting | bytes 2097152

commit v8 on v7

--- a/solution.py
+++ b/solution.py
@@ -628,11 +628,11 @@
     heads_wait(1, 1, None, 8)
     heads_to(1, 1, 0, 2, 3)
     pump_group(1, SIDES)
-    pump(1, CORNERS[0:2])
+    pump(1, CORNERS[0:1])
     heads_wait_all(256, 1)
     rows_opposite()
     emit(((turn(x, 2), 0), (turn(x, 2), 1)), 0, own_part)
-    pump(1, CORNERS[2:4])
+    pump(1, CORNERS[1:4])
     pump_group(0, ENDS)
     pump_group(0, FAR)
     pump(1, CORNERS[4:5])
@@ -650,7 +650,6 @@
         for step in steps:
             for n in range(2):
                 shrink_tile(partial.at[0], turn(z, step) * 2 + n)
-        for step in steps:
             cols = pl.ds(pl.multiple_of(turn(z, step) * 512, 512), 512)
             send_sum(partial.at[0, upper, cols], passing.at[0, :, cols], 0, 1)
             send_sum(partial.at[0, lower, cols], passing.at[1, :, cols], 0, 3)

time: 94.1 us -> 94.3 us (level)
  no operation moved by 1% of the time
where the time goes in v8:
time: 94.3 us; the launch traced here: 94.2 us
  Pallas kernels  93.2 us (99%)
  local copies, waits for them, and re-layouts  0.97 us (1%)
    pallas_call x1, Pallas kernels, local(): pl.pallas_call(layer_kernel, out_shape=pltpu.VMEM((rows, model), BF16), i...  93.2 us

profile of v8, /device:TPU:1, one launch (start us, length us, event | category | flops | bytes accessed | tf_op | source)
XLA Modules:
  0.0 94.2 jit_solution(2065717420505396012)
XLA Ops:
  0.0 93.2 %shard_map.154 = bf16[256,2048]{1,0:T(8,128)(2,1)S(1)} custom-call(bf16[256,2048]{1,0:T(8,128)(2,1)} %layer_source.1, bf16[1024,128]{1,0:T(8,128)(2,1)} %wide_query_far.1, bf16[1024,128]{1,0:T(8,128)(2,1)} %wide_forget_far.1, f32[1,128]{1,0:T(1,128)} %bitcast.13, bf16[64,1024]{1,0:T(8,128)(2,1)} %bitcast.9, bf16[64,1024]{1,0:T(8,128)(2,1)} %bitcast.10, ...), custom_call_target="tpu_custom_call" | custom-call | tf_op jit(solution)/shard_map/pallas_call | solution.py:742
  93.3 1.0 %copy.18 = bf16[256,2048]{1,0:T(8,128)(2,1)} copy(bf16[256,2048]{1,0:T(8,128)(2,1)S(1)} %shard_map.154) | data formatting | bytes 2097152
